TPU v7x, 32 devices: a whole 2x2x4 slice. The times are simulated.
32 devices in a mesh: grp: 2 (over y), sp: 4 (over z), tp: 4 (over x, core).
Axes of the slice: x: 2, y: 2, z: 4, core: 2. Of those that a mesh axis runs over, the one named last changes fastest.
Arguments:
- latents: bfloat16 [4096, 2048], P(('grp', 'sp', 'tp')), parts along dimension 0, may hold values from -6 to 6
- conv_value: bfloat16 [4096, 1024], P(('grp', 'sp'), 'tp'), parts along dimension 0, may hold values from -6 to 6
- conv_gate: bfloat16 [4096, 1024], P(('grp', 'sp'), 'tp'), parts along dimension 0, may hold values from -6 to 6
- conv_taps: float32 [31, 1024], P(None, 'tp'), may hold values from -2.2 to 2.2
- conv_gain: float32 [1024], P('tp'), may hold values from 0.1 to 1.9
- point_weight: bfloat16 [1024, 2048], P('tp'), may hold values from -0.1875 to 0.1875
- channel_gain: float32 [2048], replicated, may hold values from 0.1 to 1.9
- expert_ids: int32 [4096, 2], P(('grp', 'sp', 'tp')), parts along dimension 0, may hold values from 0 to 15, all different within a row; in each aligned block of 128 rows (0 to 127, 128 to 255, ...) at most 32 rows name the same one
- expert_weights: float32 [4096, 2], P(('grp', 'sp', 'tp')), parts along dimension 0, may hold values from 0.2 to 1
- gate_weight: bfloat16 [16, 2048, 768], P(('sp', 'tp')), may hold values from -0.125 to 0.125
- up_weight: bfloat16 [16, 2048, 768], P(('sp', 'tp')), may hold values from -0.125 to 0.125
- down_weight: bfloat16 [16, 768, 2048], P(('sp', 'tp')), may hold values from -0.21875 to 0.21875
Outputs:
- result: bfloat16 [4096, 2048], P(('grp', 'sp', 'tp')), parts along dimension 0
There are 2 independent parts, one for each index of `grp`. A program takes and returns all parts, laid end to end along the dimension named above; an argument that names none is the same for every part. Nothing has to cross between parts.
Inputs may be any that keep to these rules, and one draw needn't show every extreme that they name: `expert_ids`: each row names 2 different experts. Within the rows of one device (aligned blocks of 128 rows) no expert is named by more than 32 rows, and in some device's rows some expert is named by exactly 32.
All inputs are finite; a program needn't handle non-finite values.
Results may differ from a plain program's by a relative error of at most 0.012.
Values may be sent and summed in bfloat16 or wider, within the bound.
A program may use at most 64 MiB of HBM per device.

v0:
```python
import functools

import jax
import jax.numpy as jnp
from jax import lax
from jax.experimental import pallas as pl
from jax.experimental.pallas import tpu as pltpu
from jax.sharding import PartitionSpec as P


MESH = pl.DeviceIdType.MESH
CHUNKS = 8


def expert_kernel(
    n, tp, cap, x_hbm, tab_hbm, after_ref, wg_hbm, wu_hbm, wd_hbm, out_ref,
    toks, tabs, comp, arr, back, inc, acc, wg, wu, wd, hid,
    own_sem, w_sem, tok_send, tok_recv, tab_send, tab_recv,
    piece_send, piece_recv, back_send, back_recv, sum_send, sum_recv,
):
    z = lax.axis_index("sp")
    t = lax.axis_index("tp")
    rows, width = after_ref.shape
    slots = tp * cap
    hidden_width = wg.shape[1]
    part_rows = rows // CHUNKS
    own_tok = pltpu.make_async_copy(x_hbm, toks.at[z], own_sem.at[0])
    own_tab = pltpu.make_async_copy(tab_hbm, tabs.at[z], own_sem.at[1])
    own_tok.start()
    own_tab.start()
    loads = [
        pltpu.make_async_copy(a, b, w_sem.at[i])
        for i, (a, b) in enumerate(((wg_hbm.at[0], wg), (wu_hbm.at[0], wu), (wd_hbm.at[0], wd)))
    ]
    for load in loads:
        load.start()

    barrier = pltpu.get_barrier_semaphore()
    for p in range(1, tp):
        pl.semaphore_signal(
            barrier, inc=1, device_id={"tp": lax.rem(t + p, tp)}, device_id_type=MESH
        )

    @pl.when(z > 0)
    def _():
        pl.semaphore_signal(barrier, inc=1, device_id={"sp": z - 1}, device_id_type=MESH)

    @pl.when(z < n - 1)
    def _():
        pl.semaphore_signal(barrier, inc=1, device_id={"sp": z + 1}, device_id_type=MESH)

    peers = tp - 1 + (z > 0).astype(jnp.int32) + (z < n - 1).astype(jnp.int32)
    pl.semaphore_wait(barrier, peers)

    own_tok.wait()
    own_tab.wait()

    def source(j):
        low = jnp.minimum(z, n - 1 - z)
        near = jnp.where(j % 2 == 1, z - (j + 1) // 2, z + j // 2)
        far = jnp.where(z > n - 1 - z, z - (j - low), z + (j - low))
        return jnp.where(j <= 2 * low, near, far)

    def token_copies(zs, side):
        target = z + 1 if side else z - 1
        return [
            pltpu.make_async_remote_copy(
                src_ref=ref.at[zs],
                dst_ref=ref.at[zs],
                send_sem=ss.at[side, zs],
                recv_sem=rs.at[zs],
                device_id={"sp": target},
                device_id_type=MESH,
            )
            for ref, ss, rs in ((tabs, tab_send, tab_recv), (toks, tok_send, tok_recv))
        ]

    def span(index):
        return pl.ds(pl.multiple_of(index * cap, 16), cap)

    def exchange(j, to_ref, zs, ss, rs):
        page = lax.rem(j, 2)
        for p in range(1, tp):
            other = lax.rem(t + p, tp)
            pltpu.make_async_remote_copy(
                src_ref=comp.at[page, span(other)],
                dst_ref=to_ref.at[zs, span(t)],
                send_sem=ss.at[zs],
                recv_sem=rs.at[zs],
                device_id={"tp": other},
                device_id_type=MESH,
            ).start()
        to_ref[zs, span(t)] = comp[page, span(t)]

    def wait_pieces(ref, zs, ss, rs):
        part = ref.at[zs, pl.ds(0, (tp - 1) * cap)]
        pltpu.make_async_copy(part, part, rs.at[zs]).wait()
        pltpu.make_async_copy(part, part, ss.at[zs]).wait()

    def sum_copy(zs, k, side):
        target = z + 1 if side else z - 1
        slot = jnp.where(target == zs, n, zs) if side else zs
        piece = pl.ds(k * part_rows, part_rows)
        return pltpu.make_async_remote_copy(
            src_ref=toks.at[zs, piece],
            dst_ref=inc.at[slot, piece],
            send_sem=sum_send.at[zs, k],
            recv_sem=sum_recv.at[slot, k],
            device_id={"sp": target},
            device_id_type=MESH,
        )

    def names(zs):
        table = tabs[zs]
        base = (z * slots).astype(jnp.float32)
        place = lax.broadcasted_iota(jnp.int32, (slots, rows), 0).astype(jnp.float32) + base
        return place == table[0:1, :], place == table[1:2, :], table

    def passes_on(zs):
        return ((zs <= z) & (z < n - 1)) | ((zs >= z) & (z > 0))

    def arrive(zs):
        pltpu.make_async_copy(tabs.at[zs], tabs.at[zs], tab_recv.at[zs]).wait()
        pltpu.make_async_copy(toks.at[zs], toks.at[zs], tok_recv.at[zs]).wait()

    def forward(zs):
        @pl.when((zs <= z) & (z < n - 1))
        def _():
            for copy in token_copies(zs, 1):
                copy.start()

        @pl.when((zs >= z) & (z > 0))
        def _():
            for copy in token_copies(zs, 0):
                copy.start()

    def hand_on(j):
        zs = source(j)

        @pl.when((j < n) & passes_on(zs))
        def _():
            arrive(zs)
            forward(zs)

    def take(j):
        zs = source(j)

        @pl.when((j > 0) & jnp.logical_not(passes_on(zs)))
        def _():
            arrive(zs)

        first, second, _ = names(zs)
        pick = jnp.where(first | second, 1.0, 0.0).astype(jnp.bfloat16)
        comp[lax.rem(j, 2)] = jnp.dot(pick, toks[zs], preferred_element_type=jnp.float32).astype(jnp.bfloat16)
        exchange(j, arr, zs, piece_send, piece_recv)

    def run(j):
        zs = source(j)

        @pl.when(j == 0)
        def _():
            for load in loads:
                load.wait()

        wait_pieces(arr, zs, piece_send, piece_recv)
        step = 256
        for f in range(0, hidden_width, step):
            gate = jnp.dot(arr[zs], wg[:, f : f + step], preferred_element_type=jnp.float32)
            up = jnp.dot(arr[zs], wu[:, f : f + step], preferred_element_type=jnp.float32)
            hid[:, f : f + step] = (jax.nn.silu(gate) * up).astype(jnp.bfloat16)
        step = 512
        for c in range(0, width, step):
            comp[lax.rem(j, 2), :, c : c + step] = jnp.dot(
                hid[...], wd[:, c : c + step], preferred_element_type=jnp.float32
            ).astype(jnp.bfloat16)
        exchange(j, back, zs, back_send, back_recv)

    def merge(j):
        zs = source(j)
        wait_pieces(back, zs, back_send, back_recv)
        first, second, table = names(zs)
        share = jnp.where(first, table[2:3, :], 0.0) + jnp.where(second, table[3:4, :], 0.0)
        share = share.T
        high = share.astype(jnp.bfloat16)
        rest = (share - high.astype(jnp.float32)).astype(jnp.bfloat16)

        def total():
            return jnp.dot(high, back[zs], preferred_element_type=jnp.float32) + jnp.dot(
                rest, back[zs], preferred_element_type=jnp.float32
            )

        @pl.when((zs <= z) & (z < n - 1))
        def _():
            for copy in token_copies(zs, 1):
                copy.wait_send()

        @pl.when((zs >= z) & (z > 0))
        def _():
            for copy in token_copies(zs, 0):
                copy.wait_send()

        value = total()

        @pl.when(zs == z)
        def _():
            acc[...] = value

        @pl.when(zs != z)
        def _():
            toks[zs] = value.astype(jnp.bfloat16)

        @pl.when((zs < z) & (z == n - 1))
        def _():
            for k in range(CHUNKS):
                sum_copy(zs, k, 0).start()

        @pl.when((zs > z) & (z == 0))
        def _():
            for k in range(CHUNKS):
                sum_copy(zs, k, 1).start()

    forward(z)

    def body(j, carry):
        @pl.when(j > 0)
        def _():
            run(j - 1)

        @pl.when(j == 1)
        def _():
            hand_on(j)

        @pl.when(j > 0)
        def _():
            hand_on(j + 1)

        @pl.when(j < n)
        def _():
            take(j)

        @pl.when(j > 0)
        def _():
            merge(j - 1)

        return carry

    lax.fori_loop(0, n + 1, body, 0)

    def relay(side):
        def one(d, carry):
            zs = z + d if side else z - d

            @pl.when((zs <= n - 1) if side else (zs >= 0))
            def _():
                for k in range(CHUNKS):
                    piece = pl.ds(k * part_rows, part_rows)
                    spot = inc.at[zs, piece]
                    pltpu.make_async_copy(spot, spot, sum_recv.at[zs, k]).wait()
                    toks[zs, piece] = (
                        toks[zs, piece].astype(jnp.float32) + inc[zs, piece].astype(jnp.float32)
                    ).astype(jnp.bfloat16)
                    sum_copy(zs, k, side).start()

            return carry

        lax.fori_loop(1, n - 1, one, 0)

    upper = z > n - 1 - z

    @pl.when(upper & (z < n - 1))
    def _():
        relay(0)

    @pl.when(z > 0)
    def _():
        relay(1)

    @pl.when((z <= n - 1 - z) & (z < n - 1))
    def _():
        relay(0)

    for k in range(CHUNKS):
        piece = pl.ds(k * part_rows, part_rows)

        @pl.when(z < n - 1)
        def _():
            spot = inc.at[z, piece]
            pltpu.make_async_copy(spot, spot, sum_recv.at[z, k]).wait()
            acc[piece] = acc[piece] + inc[z, piece].astype(jnp.float32)

        @pl.when(z > 0)
        def _():
            spot = inc.at[n, piece]
            pltpu.make_async_copy(spot, spot, sum_recv.at[n, k]).wait()
            acc[piece] = acc[piece] + inc[n, piece].astype(jnp.float32)

        out_ref[piece] = (after_ref[piece].astype(jnp.float32) + acc[piece]).astype(jnp.bfloat16)

    def drain(zs, carry):
        @pl.when(zs != z)
        def _():
            for k in range(CHUNKS):
                spot = toks.at[zs, pl.ds(k * part_rows, part_rows)]
                pltpu.make_async_copy(spot, spot, sum_send.at[zs, k]).wait()

        return carry

    lax.fori_loop(0, n, drain, 0)


def experts_and_back(expert_in, table, after, gate_weight, up_weight, down_weight, cap):
    n, tp = lax.axis_size("sp"), lax.axis_size("tp")
    rows, width = expert_in.shape
    hidden_width = gate_weight.shape[2]
    slots = tp * cap
    dma = pltpu.SemaphoreType.DMA
    bf16, f32 = jnp.bfloat16, jnp.float32
    anywhere = pl.BlockSpec(memory_space=pl.ANY)
    vmem = pl.BlockSpec(memory_space=pltpu.VMEM)
    return pl.pallas_call(
        functools.partial(expert_kernel, n, tp, cap),
        out_shape=jax.ShapeDtypeStruct((rows, width), bf16),
        in_specs=[anywhere, anywhere, vmem, anywhere, anywhere, anywhere],
        out_specs=vmem,
        scratch_shapes=[
            pltpu.VMEM((n, rows, width), bf16),
            pltpu.VMEM((n,) + table.shape, f32),
            pltpu.VMEM((2, slots, width), bf16),
            pltpu.VMEM((n, slots, width), bf16),
            pltpu.VMEM((n, slots, width), bf16),
            pltpu.VMEM((n + 1, rows, width), bf16),
            pltpu.VMEM((rows, width), f32),
            pltpu.VMEM((width, hidden_width), bf16),
            pltpu.VMEM((width, hidden_width), bf16),
            pltpu.VMEM((hidden_width, width), bf16),
            pltpu.VMEM((slots, hidden_width), bf16),
            dma((2,)),
            dma((3,)),
            dma((2, n)),
            dma((n,)),
            dma((2, n)),
            dma((n,)),
            dma((n,)),
            dma((n,)),
            dma((n,)),
            dma((n,)),
            dma((n, CHUNKS)),
            dma((n + 1, CHUNKS)),
        ],
        compiler_params=pltpu.CompilerParams(
            collective_id=0, has_side_effects=True, vmem_limit_bytes=67043328
        ),
        name="experts",
    )(expert_in, table, after, gate_weight, up_weight, down_weight)


def branch_kernel(
    n, tp, taps_count, room, value_hbm, gate_hbm, taps_ref, weight_hbm, latent_hbm, gain_ref,
    ids_ref, share_ref, after_ref, in_ref, table_ref,
    value_ref, gate_ref, latent_ref, load_sem, gated, win, low, high, taps, wide, mixed, act, weights, total,
    win_send, win_recv, halo_send, halo_recv, tap_send, tap_recv, w_send, w_pass, w_recv,
):
    z = lax.axis_index("sp")
    t = lax.axis_index("tp")
    block, chans = value_ref.shape
    rows, width = latent_ref.shape
    edge = low.shape[1]
    half = taps_count // 2
    view = rows + 2 * edge
    mate = t + 1 - 2 * lax.rem(t, 2)
    halves = chans // 2
    loads = [
        pltpu.make_async_copy(a, b, load_sem.at[i])
        for i, (a, b) in enumerate(
            (
                (value_hbm, value_ref),
                (gate_hbm, gate_ref),
                (weight_hbm, weights.at[t]),
                (latent_hbm, latent_ref),
            )
        )
    ]
    for load in loads:
        load.start()

    barrier = pltpu.get_barrier_semaphore()
    for p in range(tp):
        other = lax.rem(t + p, tp)
        if p:
            pl.semaphore_signal(barrier, inc=1, device_id={"tp": other}, device_id_type=MESH)

        @pl.when(z > 0)
        def _():
            pl.semaphore_signal(
                barrier, inc=1, device_id={"sp": z - 1, "tp": other}, device_id_type=MESH
            )

        @pl.when(z < n - 1)
        def _():
            pl.semaphore_signal(
                barrier, inc=1, device_id={"sp": z + 1, "tp": other}, device_id_type=MESH
            )

    gated[pl.ds(0, edge)] = jnp.zeros((edge, chans), jnp.bfloat16)
    gated[pl.ds(edge + block, edge)] = jnp.zeros((edge, chans), jnp.bfloat16)
    loads[0].wait()
    loads[1].wait()
    step = 64
    for r in range(0, block, step):
        value = value_ref[pl.ds(r, step)].astype(jnp.float32)
        gate = gate_ref[pl.ds(r, step)].astype(jnp.float32)
        gated[pl.ds(edge + r, step)] = (value * jax.nn.sigmoid(gate)).astype(jnp.bfloat16)

    peers = tp - 1 + tp * ((z > 0).astype(jnp.int32) + (z < n - 1).astype(jnp.int32))
    pl.semaphore_wait(barrier, peers)

    def span(index):
        return pl.ds(pl.multiple_of(index * rows, 16), view)

    def win_copy(p):
        other = lax.rem(t + p, tp)
        return pltpu.make_async_remote_copy(
            src_ref=gated.at[span(other)], dst_ref=win.at[t],
            send_sem=win_send.at[p], recv_sem=win_recv.at[t],
            device_id={"tp": other}, device_id_type=MESH,
        )

    def tap_copy(p):
        other = lax.rem(t + p, tp)
        return pltpu.make_async_remote_copy(
            src_ref=taps_ref, dst_ref=taps.at[t],
            send_sem=tap_send.at[p], recv_sem=tap_recv.at[t],
            device_id={"tp": other}, device_id_type=MESH,
        )

    def halo_copy(up):
        start = block if up else edge
        place = low if up else high
        return pltpu.make_async_remote_copy(
            src_ref=gated.at[pl.ds(start, edge)], dst_ref=place.at[t],
            send_sem=halo_send.at[up], recv_sem=halo_recv.at[up, t],
            device_id={"sp": z + 1 if up else z - 1, "tp": jnp.int32(0 if up else tp - 1)},
            device_id_type=MESH,
        )

    @pl.when(z < n - 1)
    def _():
        halo_copy(1).start()

    @pl.when(z > 0)
    def _():
        halo_copy(0).start()

    for p in range(1, tp):
        win_copy(p).start()
        tap_copy(p).start()

    loads[2].wait()

    def weight_copy(source, part, target, send_sem):
        spot = pl.ds(part * halves, halves)
        return pltpu.make_async_remote_copy(
            src_ref=weights.at[source, spot],
            dst_ref=weights.at[source, spot],
            send_sem=send_sem, recv_sem=w_recv.at[source, part],
            device_id={"tp": target}, device_id_type=MESH,
        )

    def own_weights():
        copies = []
        for part in range(2):
            for q in range(1, tp // 2):
                copies.append(
                    weight_copy(t, part, lax.rem(t + 2 * q, tp), w_send.at[q, part])
                )
            copies.append(weight_copy(t, part, mate, w_send.at[0, part]))
        return copies

    for copy in own_weights():
        copy.start()

    win[t] = gated[span(t)]
    taps[t] = taps_ref[...]

    top_count = ids_ref.shape[1]
    spread_out = [
        jnp.broadcast_to(ids_ref[:, k : k + 1].astype(jnp.float32), (rows, rows))
        for k in range(top_count)
    ]
    across = [value.T for value in spread_out]
    down_place = lax.broadcasted_iota(jnp.int32, (rows, rows), 0)
    across_place = lax.broadcasted_iota(jnp.int32, (rows, rows), 1)
    table_ref[...] = jnp.zeros_like(table_ref)
    for k in range(top_count):
        count = jnp.zeros((1, rows), jnp.float32)
        for m in range(k + 1):
            same = spread_out[m] == across[k]
            if m == k:
                same = same & (down_place < across_place)
            count = count + jnp.sum(jnp.where(same, 1.0, 0.0), axis=0, keepdims=True)
        table_ref[pl.ds(k, 1)] = across[k][0:1] * room + count
        table_ref[pl.ds(top_count + k, 1)] = jnp.broadcast_to(
            share_ref[:, k : k + 1], (rows, rows)
        ).T[0:1]


    for p in range(1, tp):
        other = lax.rem(t + p, tp)
        pltpu.make_async_copy(win.at[other], win.at[other], win_recv.at[other]).wait()
        pltpu.make_async_copy(taps.at[other], taps.at[other], tap_recv.at[other]).wait()

    @pl.when((t == 0) & (z > 0))
    def _():
        for s in range(tp):
            pltpu.make_async_copy(low.at[s], low.at[s], halo_recv.at[1, s]).wait()
            win[s, pl.ds(0, edge)] = low[s]

    @pl.when((t == tp - 1) & (z < n - 1))
    def _():
        for s in range(tp):
            pltpu.make_async_copy(high.at[s], high.at[s], halo_recv.at[0, s]).wait()
            win[s, pl.ds(edge + rows, edge)] = high[s]

    def convolve(s, carry):
        first, second = carry
        wide[...] = win[s].astype(jnp.float32)
        tile = 64
        sums, squares = [], []
        for r in range(0, rows, tile):
            value = jnp.zeros((tile, chans), jnp.float32)
            for i in range(taps_count):
                value = value + taps[s, pl.ds(i, 1)] * wide[pl.ds(edge - half + i + r, tile)]
            mixed[s, pl.ds(r, tile)] = value
            sums.append(jnp.sum(value, axis=1, keepdims=True))
            squares.append(jnp.sum(value * value, axis=1, keepdims=True))
        return first + jnp.concatenate(sums, axis=0), second + jnp.concatenate(squares, axis=0)

    zero = jnp.zeros((rows, 1), jnp.float32)
    sums, squares = lax.fori_loop(0, tp, convolve, (zero, zero))
    center = sums / (chans * tp)
    spread = squares / (chans * tp) - center * center
    scale = lax.rsqrt(spread + 0.05)

    def activate(s, carry):
        value = (mixed[s] - center) * scale * taps[s, pl.ds(taps_count, 1)]
        act[s] = jax.nn.silu(value).astype(jnp.bfloat16)
        return carry

    lax.fori_loop(0, tp, activate, 0)

    def multiply(source):
        for c in range(0, width, 512):
            spot = pl.ds(c, 512)
            total[:, spot] += jnp.dot(
                act[source], weights[source, :, spot], preferred_element_type=jnp.float32
            )

    def landed(source):
        for part in range(2):
            spot = weights.at[source, pl.ds(part * halves, halves)]
            pltpu.make_async_copy(spot, spot, w_recv.at[source, part]).wait()

    loads[3].wait()
    total[...] = latent_ref[...].astype(jnp.float32)
    multiply(t)
    landed(mate)
    multiply(mate)

    def passing(q, part):
        source = lax.rem(t + 2 * q, tp)
        return weight_copy(source, part, mate, w_pass.at[q, part])

    for q in range(1, tp // 2):
        source = lax.rem(t + 2 * q, tp)
        for part in range(2):
            spot = weights.at[source, pl.ds(part * halves, halves)]
            pltpu.make_async_copy(spot, spot, w_recv.at[source, part]).wait()
            passing(q, part).start()
        multiply(source)
    for q in range(1, tp // 2):
        source = lax.rem(mate + 2 * q, tp)
        landed(source)
        multiply(source)

    for r in range(0, rows, 32):
        spot = pl.ds(r, 32)
        after = total[spot].astype(jnp.bfloat16)
        after_ref[spot] = after
        after = after.astype(jnp.float32)
        norm = lax.rsqrt(jnp.mean(after * after, axis=1, keepdims=True) + 0.01)
        in_ref[spot] = (after * norm * gain_ref[...]).astype(jnp.bfloat16)

    for p in range(1, tp):
        win_copy(p).wait_send()
        tap_copy(p).wait_send()
    for copy in own_weights():
        copy.wait_send()
    for q in range(1, tp // 2):
        for part in range(2):
            passing(q, part).wait_send()

    @pl.when(z < n - 1)
    def _():
        halo_copy(1).wait_send()

    @pl.when(z > 0)
    def _():
        halo_copy(0).wait_send()


def branch_and_norm(
    value, gate, conv_taps, conv_gain, point_weight, latents, channel_gain, ids, shares, room
):
    n, tp = lax.axis_size("sp"), lax.axis_size("tp")
    block, chans = value.shape
    rows, width = latents.shape
    taps_count = conv_taps.shape[0]
    edge = -(-(taps_count // 2) // 16) * 16
    table = jnp.concatenate([conv_taps, conv_gain[None, :]], axis=0)
    table = jnp.pad(table, ((0, -table.shape[0] % 8), (0, 0)))
    dma = pltpu.SemaphoreType.DMA
    bf16, f32 = jnp.bfloat16, jnp.float32
    anywhere = pl.BlockSpec(memory_space=pl.ANY)
    vmem = pl.BlockSpec(memory_space=pltpu.VMEM)
    return pl.pallas_call(
        functools.partial(branch_kernel, n, tp, taps_count, room),
        out_shape=[jax.ShapeDtypeStruct((rows, width), bf16)] * 2
        + [jax.ShapeDtypeStruct((8, rows), f32)],
        in_specs=[anywhere, anywhere, vmem, anywhere, anywhere, vmem, vmem, vmem],
        out_specs=[vmem] * 3,
        scratch_shapes=[
            pltpu.VMEM((block, chans), bf16),
            pltpu.VMEM((block, chans), bf16),
            pltpu.VMEM((rows, width), bf16),
            dma((4,)),
            pltpu.VMEM((block + 2 * edge, chans), bf16),
            pltpu.VMEM((tp, rows + 2 * edge, chans), bf16),
            pltpu.VMEM((tp, edge, chans), bf16),
            pltpu.VMEM((tp, edge, chans), bf16),
            pltpu.VMEM((tp,) + table.shape, f32),
            pltpu.VMEM((rows + 2 * edge, chans), f32),
            pltpu.VMEM((tp, rows, chans), f32),
            pltpu.VMEM((tp, rows, chans), bf16),
            pltpu.VMEM((tp, chans, width), bf16),
            pltpu.VMEM((rows, width), f32),
            dma((tp,)),
            dma((tp,)),
            dma((2,)),
            dma((2, tp)),
            dma((tp,)),
            dma((tp,)),
            dma((tp // 2, 2)),
            dma((tp // 2, 2)),
            dma((tp, 2)),
        ],
        compiler_params=pltpu.CompilerParams(
            collective_id=1, has_side_effects=True, vmem_limit_bytes=67043328
        ),
        name="branch",
    )(value, gate, table, point_weight, latents, channel_gain[None, :], ids, shares)


def shards(
    latents,
    conv_value,
    conv_gate,
    conv_taps,
    conv_gain,
    point_weight,
    channel_gain,
    expert_ids,
    expert_weights,
    gate_weight,
    up_weight,
    down_weight,
):
    row_count, top_count = expert_ids.shape
    experts = gate_weight.shape[0] * lax.axis_size(("sp", "tp"))
    capacity = 2 * top_count * row_count // experts
    room = -(-capacity // 16) * 16
    after, expert_in, table = branch_and_norm(
        conv_value, conv_gate, conv_taps, conv_gain, point_weight, latents, channel_gain,
        expert_ids, expert_weights, room,
    )
    return experts_and_back(
        expert_in, table, after, gate_weight, up_weight, down_weight, room
    )


def solution(mesh):
    return jax.shard_map(
        shards,
        mesh=mesh,
        in_specs=(
            P(("grp", "sp", "tp"), None),
            P(("grp", "sp"), "tp"),
            P(("grp", "sp"), "tp"),
            P(None, "tp"),
            P("tp"),
            P("tp", None),
            P(),
            P(("grp", "sp", "tp"), None),
            P(("grp", "sp", "tp"), None),
            P(("sp", "tp"), None, None),
            P(("sp", "tp"), None, None),
            P(("sp", "tp"), None, None),
        ),
        out_specs=P(("grp", "sp", "tp"), None),
        check_vma=False,
    )
```

profile of v0, /device:TPU:0, one launch (start us, length us, event | category | flops | bytes accessed | tf_op | source)
XLA Modules:
  0.0 133.9 jit_solution(16187107089058798683)
XLA Ops:
  0.0 1.4 %pad_maximum_fusion.taps_ref = f32[32,256]{1,0:T(8,128)} fusion(f32[1,256]{1,0:T(1,128)} %bitcast.3, f32[31,256]{1,0:T(8,128)} %param.15), kind=kLoop, calls=%fused_computation | loop fusion | flops 8192 | bytes 65536 | tf_op jit(solution)/shard_map/concatenate | solution.py:619
  1.4 1.4 %copy.13.ids_ref = s32[128,2]{1,0:T(8,128)} copy(s32[128,2]{0,1:T(2,128)} %param.19) | data formatting | bytes 2048 | tf_op args[7]
  2.8 1.4 %copy.14.share_ref = f32[128,2]{1,0:T(8,128)} copy(f32[128,2]{0,1:T(2,128)} %param.20) | data formatting | bytes 2048 | tf_op args[8]
  4.2 36.7 %branch.1 = (bf16[128,2048]{1,0:T(8,128)(2,1)}, bf16[128,2048]{1,0:T(8,128)(2,1)}, f32[8,128]{1,0:T(8,128)}) custom-call(bf16[512,256]{1,0:T(8,128)(2,1)} %value_hbm.1, bf16[512,256]{1,0:T(8,128)(2,1)} %gate_hbm.1, f32[32,256]{1,0:T(8,128)} %pad_maximum_fusion.taps_ref, bf16[256,2048]{1,0:T(8,128)(2,1)} %weight_hbm.1, bf16[128,2048]{1,0:T(8,128)(2,1)} %latent_hbm.1, ...), custom_call_target="tpu_custom_call" | custom-call | tf_op jit(solution)/shard_map/branch/pallas_call | solution.py:625
  41.0 91.0 %experts.1 = bf16[128,2048]{1,0:T(8,128)(2,1)} custom-call(bf16[128,2048]{1,0:T(8,128)(2,1)} %get-tuple-element.8.x_hbm, f32[8,128]{1,0:T(8,128)} %get-tuple-element.9.tab_hbm, bf16[128,2048]{1,0:T(8,128)(2,1)} %get-tuple-element.10.after_ref, bf16[1,2048,768]{2,1,0:T(8,128)(2,1)} %wg_hbm.1, bf16[1,2048,768]{2,1,0:T(8,128)(2,1)} %wu_hbm.1, ...), custom_call_target="tpu_custom_call" | custom-call | tf_op jit(solution)/shard_map/experts/pallas_call | solution.py:320
  132.0 1.9 %copy.16 = bf16[128,2048]{1,0:T(8,128)(2,1)} copy(bf16[128,2048]{1,0:T(8,128)(2,1)} %experts.1) | data formatting | bytes 1048576
where the time goes:
time: 134 us
  Pallas kernels  128 us (96%)
  local copies, waits for them, and re-layouts  4.71 us (4%)
  other arithmetic  1.39 us (1%)
    pallas_call x1, Pallas kernels, experts_and_back(): pl.pallas_call(functools.partial(expert_kernel, n, tp, cap), out_shape=ja...  91 us
    pallas_call x1, Pallas kernels, branch_and_norm(): pl.pallas_call(functools.partial(branch_kernel, n, tp, taps_count, room),...  36.7 us
    unnamed x3, local copies, waits for them, and re-layouts  4.71 us

commit v1 on v0

v1 whole, which is shorter than its diff:
```python
import functools

import jax
import jax.numpy as jnp
from jax import lax
from jax.experimental import pallas as pl
from jax.experimental.pallas import tpu as pltpu
from jax.sharding import PartitionSpec as P


MESH = pl.DeviceIdType.MESH
PARTS = 4
BANDS = 4


def layer_kernel(
    n, tp, taps_count, cap,
    value_hbm, gate_hbm, taps_hbm, cgain_hbm, weight_hbm, latent_hbm, gain_hbm, ids_hbm, share_hbm,
    wg_hbm, wu_hbm, wd_hbm, out_ref,
    value_ref, gate_ref, taps_ref, cgain_ref, gain_ref, ids_ref, share_ref,
    gated, wide, mixed, stats, act_out, act_in, psend,
    toks, tabs, comp, arr, back, inc, acc, wg, wu, wd, ga, ua, hid,
    load_sem, point_sem, w_sem, halo_send, halo_recv, stat_send, stat_recv, mate_send, mate_recv,
    act_send, act_recv, part_send, part_recv,
    tok_send, tok_recv, tab_send, tab_recv,
    piece_send, piece_recv, back_send, back_recv, sum_send, sum_recv,
):
    z = lax.axis_index("sp")
    t = lax.axis_index("tp")
    block, chans = value_ref.shape
    rows, width = out_ref.shape
    slots = tp * cap
    hidden_width = wg.shape[1]
    top_count = ids_ref.shape[0]
    cols = width // PARTS
    band_rows = rows // BANDS
    half = taps_count // 2
    edge = (gated.shape[0] - block) // 2
    view = rows + 2 * edge
    q_count = tp // 2
    core = lax.rem(t, 2)
    quad = t // 2
    mate = t + 1 - 2 * core
    chunks = chans // rows
    base = 2 * chunks

    def col(c):
        return pl.ds(c * cols, cols)

    loads = [
        pltpu.make_async_copy(a, b, load_sem.at[i])
        for i, (a, b) in enumerate(
            (
                (value_hbm, value_ref),
                (gate_hbm, gate_ref),
                (taps_hbm, taps_ref),
                (cgain_hbm, cgain_ref),
                (ids_hbm, ids_ref),
                (share_hbm, share_ref),
                (gain_hbm, gain_ref),
                (latent_hbm, out_ref),
            )
        )
    ]
    for load in loads:
        load.start()

    point_loads = [
        pltpu.make_async_copy(
            weight_hbm.at[pl.ds(b * rows, rows), col(c)],
            inc.at[core * chunks + b, c],
            point_sem.at[b, c],
        )
        for b in range(chunks)
        for c in range(PARTS)
    ]
    for load in point_loads:
        load.start()

    barrier = pltpu.get_barrier_semaphore()
    for p in range(1, tp):
        pl.semaphore_signal(
            barrier, inc=1, device_id={"tp": lax.rem(t + p, tp)}, device_id_type=MESH
        )

    @pl.when(z > 0)
    def _():
        pl.semaphore_signal(barrier, inc=1, device_id={"sp": z - 1}, device_id_type=MESH)

    @pl.when(z < n - 1)
    def _():
        pl.semaphore_signal(barrier, inc=1, device_id={"sp": z + 1}, device_id_type=MESH)

    @pl.when(z == 0)
    def _():
        gated[pl.ds(0, edge)] = jnp.zeros((edge, chans), jnp.bfloat16)

    @pl.when(z == n - 1)
    def _():
        gated[pl.ds(edge + block, edge)] = jnp.zeros((edge, chans), jnp.bfloat16)

    loads[0].wait()
    loads[1].wait()
    step = 64
    for r in range(0, block, step):
        value = value_ref[pl.ds(r, step)].astype(jnp.float32)
        gate = gate_ref[pl.ds(r, step)].astype(jnp.float32)
        gated[pl.ds(edge + r, step)] = (value * jax.nn.sigmoid(gate)).astype(jnp.bfloat16)

    peers = tp - 1 + (z > 0).astype(jnp.int32) + (z < n - 1).astype(jnp.int32)
    pl.semaphore_wait(barrier, peers)

    def halo_copy(up):
        start = block if up else edge
        place = 0 if up else edge + block
        return pltpu.make_async_remote_copy(
            src_ref=gated.at[pl.ds(start, edge)], dst_ref=gated.at[pl.ds(place, edge)],
            send_sem=halo_send.at[up], recv_sem=halo_recv.at[up],
            device_id={"sp": z + 1 if up else z - 1}, device_id_type=MESH,
        )

    @pl.when(z < n - 1)
    def _():
        halo_copy(1).start()

    @pl.when(z > 0)
    def _():
        halo_copy(0).start()

    for load in point_loads:
        load.wait()
    own_rows = pl.ds(core * chunks, chunks)
    mate_copy = pltpu.make_async_remote_copy(
        src_ref=inc.at[own_rows], dst_ref=inc.at[own_rows],
        send_sem=mate_send.at[0], recv_sem=mate_recv.at[0],
        device_id={"tp": mate}, device_id_type=MESH,
    )
    mate_copy.start()

    expert_loads = [
        pltpu.make_async_copy(a, b, w_sem.at[i])
        for i, (a, b) in enumerate(((wg_hbm.at[0], wg), (wu_hbm.at[0], wu), (wd_hbm.at[0], wd)))
    ]
    for load in expert_loads:
        load.start()
    for load in loads[2:]:
        load.wait()

    def convolve(s):
        wide[...] = gated[pl.ds(pl.multiple_of(s * rows, 16), view)].astype(jnp.float32)
        tile = 64
        sums, squares = [], []
        for r in range(0, rows, tile):
            value = jnp.zeros((tile, chans), jnp.float32)
            for i in range(taps_count):
                value = value + taps_ref[pl.ds(i, 1)] * wide[pl.ds(edge - half + i + r, tile)]
            mixed[s, pl.ds(r, tile)] = value
            sums.append(jnp.sum(value, axis=1, keepdims=True))
            squares.append(jnp.sum(value * value, axis=1, keepdims=True))
        for k, parts in enumerate((sums, squares)):
            line = jnp.broadcast_to(jnp.concatenate(parts, axis=0), (rows, rows)).T
            stats[t, s, pl.ds(k, 1)] = line[0:1]

    def inner(i, carry):
        convolve(i + 1)
        return carry

    lax.fori_loop(0, tp - 2, inner, 0)

    @pl.when(z > 0)
    def _():
        halo_copy(1).wait_recv()

    @pl.when(z < n - 1)
    def _():
        halo_copy(0).wait_recv()

    def outer(i, carry):
        convolve(i * (tp - 1))
        return carry

    lax.fori_loop(0, 2, outer, 0)

    def stat_copy(p):
        return pltpu.make_async_remote_copy(
            src_ref=stats.at[t], dst_ref=stats.at[t],
            send_sem=stat_send.at[p], recv_sem=stat_recv.at[t],
            device_id={"tp": lax.rem(t + p, tp)}, device_id_type=MESH,
        )

    for p in range(1, tp):
        stat_copy(p).start()

    ids = ids_ref[...].astype(jnp.float32)
    across = [jnp.broadcast_to(ids[k : k + 1], (rows, rows)) for k in range(top_count)]
    down = [value.T for value in across]
    down_place = lax.broadcasted_iota(jnp.int32, (rows, rows), 0)
    across_place = lax.broadcasted_iota(jnp.int32, (rows, rows), 1)
    tabs[z] = jnp.zeros(tabs.shape[1:], jnp.float32)
    for k in range(top_count):
        count = jnp.zeros((1, rows), jnp.float32)
        for m in range(k + 1):
            same = down[m] == across[k]
            if m == k:
                same = same & (down_place < across_place)
            count = count + jnp.sum(jnp.where(same, 1.0, 0.0), axis=0, keepdims=True)
        tabs[z, pl.ds(k, 1)] = ids[k : k + 1] * cap + count
        tabs[z, pl.ds(top_count + k, 1)] = share_ref[pl.ds(k, 1)]

    for p in range(1, tp):
        other = lax.rem(t + p, tp)
        pltpu.make_async_copy(stats.at[other], stats.at[other], stat_recv.at[other]).wait()

    def activate(s):
        both = stats[0, s]
        for p in range(1, tp):
            both = both + stats[p, s]
        both = both / (chans * tp)
        center = both[0:1]
        scale = lax.rsqrt(both[1:2] - center * center + 0.05)
        center = jnp.broadcast_to(center, (rows, rows)).T[:, 0:1]
        scale = jnp.broadcast_to(scale, (rows, rows)).T[:, 0:1]
        value = (mixed[s] - center) * scale * cgain_ref[...]
        return jax.nn.silu(value).astype(jnp.bfloat16)

    def act_copy(i):
        spot = lax.rem(quad + i, q_count)
        return pltpu.make_async_remote_copy(
            src_ref=act_out.at[spot], dst_ref=act_in.at[spot, core],
            send_sem=act_send.at[i], recv_sem=act_recv.at[spot],
            device_id={"tp": mate}, device_id_type=MESH,
        )

    order = list(range(1, q_count)) + [0]
    for i in order:
        spot = lax.rem(quad + i, q_count)
        act_out[spot] = activate(2 * spot + 1 - core)
        act_copy(i).start()
    for i in order:
        spot = lax.rem(quad + i, q_count)
        act_in[spot, core] = activate(2 * spot + core)

    mate_copy.wait()

    def product(i, c):
        spot = lax.rem(quad + i, q_count)
        left = jnp.concatenate([act_in[spot, 0], act_in[spot, 1]], axis=1)
        right = inc[pl.ds(0, base), c].reshape(base * rows, cols)
        return jnp.dot(left, right, preferred_element_type=jnp.float32)

    def part_copy(i, k):
        piece = pl.ds(k * band_rows, band_rows)
        return pltpu.make_async_remote_copy(
            src_ref=psend.at[i - 1, :, piece], dst_ref=inc.at[base + i - 1, :, piece],
            send_sem=part_send.at[i - 1, k], recv_sem=part_recv.at[i - 1, k],
            device_id={"tp": 2 * lax.rem(quad + i, q_count) + core}, device_id_type=MESH,
        )

    for i in order:
        spot = lax.rem(quad + i, q_count)
        pltpu.make_async_copy(act_out.at[spot], act_out.at[spot], act_recv.at[spot]).wait()
        for c in range(PARTS):
            if i:
                psend[i - 1, c] = product(i, c).astype(jnp.bfloat16)
            else:
                acc[c] = product(i, c)
        if i:
            for k in range(BANDS):
                part_copy(i, k).start()

    def token_copy(zs, k, side):
        piece = pl.ds(k * band_rows, band_rows)
        return pltpu.make_async_remote_copy(
            src_ref=toks.at[zs, :, piece], dst_ref=toks.at[zs, :, piece],
            send_sem=tok_send.at[side, zs, k], recv_sem=tok_recv.at[zs, k],
            device_id={"sp": z + 1 if side else z - 1}, device_id_type=MESH,
        )

    def table_copy(zs, side):
        return pltpu.make_async_remote_copy(
            src_ref=tabs.at[zs], dst_ref=tabs.at[zs],
            send_sem=tab_send.at[side, zs], recv_sem=tab_recv.at[zs],
            device_id={"sp": z + 1 if side else z - 1}, device_id_type=MESH,
        )

    def each_side(zs, act):
        @pl.when((zs <= z) & (z < n - 1))
        def _():
            act(1)

        @pl.when((zs >= z) & (z > 0))
        def _():
            act(0)

    each_side(z, lambda side: table_copy(z, side).start())

    for k in range(BANDS):
        piece = pl.ds(k * band_rows, band_rows)
        for i in range(1, q_count):
            spot = inc.at[base + i - 1, :, piece]
            pltpu.make_async_copy(spot, spot, part_recv.at[i - 1, k]).wait()
        square = jnp.zeros((band_rows, 1), jnp.float32)
        for c in range(PARTS):
            total = acc[c, piece] + out_ref[piece, col(c)].astype(jnp.float32)
            for i in range(1, q_count):
                total = total + inc[base + i - 1, c, piece].astype(jnp.float32)
            after = total.astype(jnp.bfloat16)
            out_ref[piece, col(c)] = after
            after = after.astype(jnp.float32)
            square = square + jnp.sum(after * after, axis=1, keepdims=True)
        norm = lax.rsqrt(square / width + 0.01)
        for c in range(PARTS):
            after = out_ref[piece, col(c)].astype(jnp.float32)
            toks[z, c, piece] = (after * norm * gain_ref[:, col(c)]).astype(jnp.bfloat16)
        each_side(z, lambda side: token_copy(z, k, side).start())


    def source(j):
        low = jnp.minimum(z, n - 1 - z)
        near = jnp.where(j % 2 == 1, z - (j + 1) // 2, z + j // 2)
        far = jnp.where(z > n - 1 - z, z - (j - low), z + (j - low))
        return jnp.where(j <= 2 * low, near, far)

    def span(index):
        return pl.ds(pl.multiple_of(index * cap, 16), cap)

    def exchange(j, c, to_ref, zs, ss, rs):
        page = lax.rem(j, 2)
        for p in range(1, tp):
            other = lax.rem(t + p, tp)
            pltpu.make_async_remote_copy(
                src_ref=comp.at[page, c, span(other)],
                dst_ref=to_ref.at[zs, c, span(t)],
                send_sem=ss.at[zs, c],
                recv_sem=rs.at[zs, c],
                device_id={"tp": other},
                device_id_type=MESH,
            ).start()
        to_ref[zs, c, span(t)] = comp[page, c, span(t)]

    def wait_pieces(ref, zs, c, ss, rs):
        part = ref.at[zs, c, pl.ds(0, (tp - 1) * cap)]
        pltpu.make_async_copy(part, part, rs.at[zs, c]).wait()
        pltpu.make_async_copy(part, part, ss.at[zs, c]).wait()

    def sum_copy(zs, c, side):
        target = z + 1 if side else z - 1
        slot = jnp.where(target == zs, n, zs) if side else zs
        return pltpu.make_async_remote_copy(
            src_ref=toks.at[zs, c],
            dst_ref=inc.at[slot, c],
            send_sem=sum_send.at[zs, c],
            recv_sem=sum_recv.at[slot, c],
            device_id={"sp": target},
            device_id_type=MESH,
        )

    def names(zs):
        table = tabs[zs]
        start = (z * slots).astype(jnp.float32)
        place = lax.broadcasted_iota(jnp.int32, (slots, rows), 0).astype(jnp.float32) + start
        return place == table[0:1, :], place == table[1:2, :], table

    def passes_on(zs):
        return ((zs < z) & (z < n - 1)) | ((zs > z) & (z > 0))

    def arrive(zs, k):
        spot = toks.at[zs, :, pl.ds(k * band_rows, band_rows)]
        pltpu.make_async_copy(spot, spot, tok_recv.at[zs, k]).wait()

    def hand_on(j):
        zs = source(jnp.minimum(j, n - 1))

        @pl.when((j < n) & passes_on(zs))
        def _():
            pltpu.make_async_copy(tabs.at[zs], tabs.at[zs], tab_recv.at[zs]).wait()
            each_side(zs, lambda side: table_copy(zs, side).start())
            for k in range(BANDS):
                arrive(zs, k)
                each_side(zs, lambda side: token_copy(zs, k, side).start())

    def take(j):
        zs = source(j)

        @pl.when((zs != z) & jnp.logical_not(passes_on(zs)))
        def _():
            pltpu.make_async_copy(tabs.at[zs], tabs.at[zs], tab_recv.at[zs]).wait()
            for k in range(BANDS):
                arrive(zs, k)

        first, second, _ = names(zs)
        pick = jnp.where(first | second, 1.0, 0.0).astype(jnp.bfloat16)
        page = lax.rem(j, 2)
        for c in range(PARTS):
            comp[page, c] = jnp.dot(
                pick, toks[zs, c], preferred_element_type=jnp.float32
            ).astype(jnp.bfloat16)
            exchange(j, c, arr, zs, piece_send, piece_recv)

    def run(j):
        zs = source(j)

        @pl.when(j == 0)
        def _():
            for load in expert_loads:
                load.wait()

        step = 256
        for c in range(PARTS):
            wait_pieces(arr, zs, c, piece_send, piece_recv)
            for f in range(0, hidden_width, step):
                for to, weights in ((ga, wg), (ua, wu)):
                    value = jnp.dot(
                        arr[zs, c], weights[col(c), f : f + step],
                        preferred_element_type=jnp.float32,
                    )
                    if c:
                        value = value + to[:, f : f + step]
                    if c < PARTS - 1 or to is ga:
                        to[:, f : f + step] = value
                if c == PARTS - 1:
                    gate = ga[:, f : f + step]
                    hid[:, f : f + step] = (jax.nn.silu(gate) * value).astype(jnp.bfloat16)
        page = lax.rem(j, 2)
        for c in range(PARTS):
            comp[page, c] = jnp.dot(
                hid[...], wd[:, col(c)], preferred_element_type=jnp.float32
            ).astype(jnp.bfloat16)
            exchange(j, c, back, zs, back_send, back_recv)

    def merge(j):
        zs = source(j)
        first, second, table = names(zs)
        share = jnp.where(first, table[2:3, :], 0.0) + jnp.where(second, table[3:4, :], 0.0)
        share = share.T
        high = share.astype(jnp.bfloat16)
        rest = (share - high.astype(jnp.float32)).astype(jnp.bfloat16)

        def sent(side):
            table_copy(zs, side).wait_send()
            for k in range(BANDS):
                token_copy(zs, k, side).wait_send()

        each_side(zs, sent)
        for c in range(PARTS):
            wait_pieces(back, zs, c, back_send, back_recv)
            value = jnp.dot(high, back[zs, c], preferred_element_type=jnp.float32) + jnp.dot(
                rest, back[zs, c], preferred_element_type=jnp.float32
            )

            @pl.when(zs == z)
            def _():
                acc[c] = value

            @pl.when(zs != z)
            def _():
                toks[zs, c] = value.astype(jnp.bfloat16)

            @pl.when((zs < z) & (z == n - 1))
            def _():
                sum_copy(zs, c, 0).start()

            @pl.when((zs > z) & (z == 0))
            def _():
                sum_copy(zs, c, 1).start()

    upper = z > n - 1 - z

    def relay(turn):
        def pass_sum(zs, side, c):
            spot = inc.at[zs, c]
            pltpu.make_async_copy(spot, spot, sum_recv.at[zs, c]).wait()
            toks[zs, c] = (
                toks[zs, c].astype(jnp.float32) + inc[zs, c].astype(jnp.float32)
            ).astype(jnp.bfloat16)
            sum_copy(zs, c, side).start()

        def go_up(c):
            @pl.when((z > 0) & (z < turn))
            def _():
                pass_sum(turn, 1, c)

        def go_down(c):
            @pl.when((z < n - 1) & (z > n - 1 - turn))
            def _():
                pass_sum(n - 1 - turn, 0, c)

        for c in range(PARTS):
            @pl.when(upper)
            def _():
                go_down(c)

            go_up(c)

            @pl.when(jnp.logical_not(upper))
            def _():
                go_down(c)

    def body(j, carry):
        @pl.when(j == 1)
        def _():
            hand_on(j)

        @pl.when(j > 0)
        def _():
            hand_on(j + 1)

        @pl.when(j < n)
        def _():
            take(j)

        @pl.when((j > 0) & (j <= n))
        def _():
            merge(j - 1)

        @pl.when(j < n)
        def _():
            run(j)

        @pl.when(j > 2)
        def _():
            relay(j - 2)

        return carry

    lax.fori_loop(0, n + 2, body, 0)

    for c in range(PARTS):
        @pl.when(z < n - 1)
        def _():
            spot = inc.at[z, c]
            pltpu.make_async_copy(spot, spot, sum_recv.at[z, c]).wait()
            acc[c] = acc[c] + inc[z, c].astype(jnp.float32)

        @pl.when(z > 0)
        def _():
            spot = inc.at[n, c]
            pltpu.make_async_copy(spot, spot, sum_recv.at[n, c]).wait()
            acc[c] = acc[c] + inc[n, c].astype(jnp.float32)

        out_ref[:, col(c)] = (out_ref[:, col(c)].astype(jnp.float32) + acc[c]).astype(jnp.bfloat16)

    def drain(zs, carry):
        @pl.when(zs != z)
        def _():
            for c in range(PARTS):
                spot = toks.at[zs, c]
                pltpu.make_async_copy(spot, spot, sum_send.at[zs, c]).wait()

        return carry

    lax.fori_loop(0, n, drain, 0)
    for p in range(1, tp):
        stat_copy(p).wait_send()
    for i in order:
        act_copy(i).wait_send()
        if i:
            for k in range(BANDS):
                part_copy(i, k).wait_send()

    @pl.when(z < n - 1)
    def _():
        halo_copy(1).wait_send()

    @pl.when(z > 0)
    def _():
        halo_copy(0).wait_send()


def shards(
    latents,
    conv_value,
    conv_gate,
    conv_taps,
    conv_gain,
    point_weight,
    channel_gain,
    expert_ids,
    expert_weights,
    gate_weight,
    up_weight,
    down_weight,
):
    n, tp = lax.axis_size("sp"), lax.axis_size("tp")
    rows, top_count = expert_ids.shape
    experts = gate_weight.shape[0] * n * tp
    cap = -(-(2 * top_count * rows // experts) // 16) * 16
    block, chans = conv_value.shape
    width = latents.shape[1]
    taps_count = conv_taps.shape[0]
    hidden_width = gate_weight.shape[2]
    slots = tp * cap
    cols = width // PARTS
    edge = -(-(taps_count // 2) // 16) * 16
    q_count = tp // 2
    spots = max(n + 1, 2 * chans // rows + q_count - 1)
    dma = pltpu.SemaphoreType.DMA
    bf16, f32 = jnp.bfloat16, jnp.float32
    anywhere = pl.BlockSpec(memory_space=pl.ANY)
    vmem = pltpu.VMEM
    return pl.pallas_call(
        functools.partial(layer_kernel, n, tp, taps_count, cap),
        out_shape=jax.ShapeDtypeStruct((rows, width), bf16),
        in_specs=[anywhere] * 12,
        out_specs=pl.BlockSpec(memory_space=pltpu.VMEM),
        scratch_shapes=[
            vmem((block, chans), bf16),
            vmem((block, chans), bf16),
            vmem((taps_count, chans), f32),
            vmem((1, chans), f32),
            vmem((1, width), f32),
            vmem((top_count, rows), jnp.int32),
            vmem((top_count, rows), f32),
            vmem((block + 2 * edge, chans), bf16),
            vmem((rows + 2 * edge, chans), f32),
            vmem((tp, rows, chans), f32),
            vmem((tp, tp, 8, rows), f32),
            vmem((q_count, rows, chans), bf16),
            vmem((q_count, 2, rows, chans), bf16),
            vmem((q_count - 1, PARTS, rows, cols), bf16),
            vmem((n, PARTS, rows, cols), bf16),
            vmem((n, 8, rows), f32),
            vmem((2, PARTS, slots, cols), bf16),
            vmem((n, PARTS, slots, cols), bf16),
            vmem((n, PARTS, slots, cols), bf16),
            vmem((spots, PARTS, rows, cols), bf16),
            vmem((PARTS, rows, cols), f32),
            vmem((width, hidden_width), bf16),
            vmem((width, hidden_width), bf16),
            vmem((hidden_width, width), bf16),
            vmem((slots, hidden_width), f32),
            vmem((slots, hidden_width), f32),
            vmem((slots, hidden_width), bf16),
            dma((8,)),
            dma((chans // rows, PARTS)),
            dma((3,)),
            dma((2,)),
            dma((2,)),
            dma((tp,)),
            dma((tp,)),
            dma((1,)),
            dma((1,)),
            dma((q_count,)),
            dma((q_count,)),
            dma((q_count - 1, BANDS)),
            dma((q_count - 1, BANDS)),
            dma((2, n, BANDS)),
            dma((n, BANDS)),
            dma((2, n)),
            dma((n,)),
            dma((n, PARTS)),
            dma((n, PARTS)),
            dma((n, PARTS)),
            dma((n, PARTS)),
            dma((n, PARTS)),
            dma((n + 1, PARTS)),
        ],
        compiler_params=pltpu.CompilerParams(
            collective_id=0, has_side_effects=True, vmem_limit_bytes=67043328
        ),
        name="layer",
    )(
        conv_value, conv_gate, conv_taps, conv_gain[None, :], point_weight, latents,
        channel_gain[None, :], expert_ids.T, expert_weights.T,
        gate_weight, up_weight, down_weight,
    )


def solution(mesh):
    return jax.shard_map(
        shards,
        mesh=mesh,
        in_specs=(
            P(("grp", "sp", "tp"), None),
            P(("grp", "sp"), "tp"),
            P(("grp", "sp"), "tp"),
            P(None, "tp"),
            P("tp"),
            P("tp", None),
            P(),
            P(("grp", "sp", "tp"), None),
            P(("grp", "sp", "tp"), None),
            P(("sp", "tp"), None, None),
            P(("sp", "tp"), None, None),
            P(("sp", "tp"), None, None),
        ),
        out_specs=P(("grp", "sp", "tp"), None),
        check_vma=False,
    )
```

time: 134 us -> 122 us (0.910)
  Pallas kernels: 128 us -> 120 us
  local copies, waits for them, and re-layouts: 4.71 us -> 1.88 us
  other arithmetic: 1.39 us -> 0 us
    pallas_call x2 -> x1, Pallas kernels: 128 us -> 120 us  [shards(): pl.pallas_call(functools.partial(layer_kernel, n, tp, taps_count, cap), o...]
    unnamed x3 -> x1, local copies, waits for them, and re-layouts: 4.71 us -> 1.88 us
    concatenate x1 -> x0, other arithmetic: 1.39 us -> none  [branch_and_norm(): table = jnp.concatenate([conv_taps, conv_gain[None, :]], axis=0)]
where the time goes in v1:
time: 122 us
  Pallas kernels  120 us (98%)
  local copies, waits for them, and re-layouts  1.88 us (2%)
    pallas_call x1, Pallas kernels, shards(): pl.pallas_call(functools.partial(layer_kernel, n, tp, taps_count, cap), o...  120 us

profile of v1, /device:TPU:0, one launch (start us, length us, event | category | flops | bytes accessed | tf_op | source)
XLA Modules:
  0.0 121.6 jit_solution(693404042377282893)
XLA Ops:
  0.0 119.7 %layer.1 = bf16[128,2048]{1,0:T(8,128)(2,1)} custom-call(bf16[512,256]{1,0:T(8,128)(2,1)} %value_hbm.1, bf16[512,256]{1,0:T(8,128)(2,1)} %gate_hbm.1, f32[31,256]{1,0:T(8,128)} %taps_hbm.1, f32[1,256]{1,0:T(1,128)} %bitcast.5, bf16[256,2048]{1,0:T(8,128)(2,1)} %weight_hbm.1, bf16[128,2048]{1,0:T(8,128)(2,1)} %latent_hbm.1, f32[1,2048]{1,0:T(1,128)} %bitcast.4, ...), custom_call_target="tpu_custom_call" | custom-call | tf_op jit(solution)/shard_map/layer/pallas_call | solution.py:601
  119.7 1.9 %copy.14 = bf16[128,2048]{1,0:T(8,128)(2,1)} copy(bf16[128,2048]{1,0:T(8,128)(2,1)} %layer.1) | data formatting | bytes 1048576

commit v2 on v1

--- a/solution.py
+++ b/solution.py
@@ -10,17 +10,20 @@
 
 MESH = pl.DeviceIdType.MESH
 PARTS = 4
-BANDS = 4
+BANDS = (0, 1, 2, 3, 4, 5, 6, 7, 8)
+SPLIT = 2
+LAG = 3
+PAGES = 3
 
 
 def layer_kernel(
     n, tp, taps_count, cap,
     value_hbm, gate_hbm, taps_hbm, cgain_hbm, weight_hbm, latent_hbm, gain_hbm, ids_hbm, share_hbm,
-    wg_hbm, wu_hbm, wd_hbm, out_ref,
+    wg_hbm, wu_hbm, wd_hbm, out_hbm,
     value_ref, gate_ref, taps_ref, cgain_ref, gain_ref, ids_ref, share_ref,
-    gated, wide, mixed, stats, act_out, act_in, psend,
+    kept, gated, wide, mixed, stats, act_out, act_in, psend,
     toks, tabs, comp, arr, back, inc, acc, wg, wu, wd, ga, ua, hid,
-    load_sem, point_sem, w_sem, halo_send, halo_recv, stat_send, stat_recv, mate_send, mate_recv,
+    load_sem, point_sem, w_sem, out_sem, halo_send, halo_recv, stat_send, stat_recv, mate_send, mate_recv,
     act_send, act_recv, part_send, part_recv,
     tok_send, tok_recv, tab_send, tab_recv,
     piece_send, piece_recv, back_send, back_recv, sum_send, sum_recv,
@@ -28,12 +31,11 @@
     z = lax.axis_index("sp")
     t = lax.axis_index("tp")
     block, chans = value_ref.shape
-    rows, width = out_ref.shape
+    rows, width = kept.shape
     slots = tp * cap
     hidden_width = wg.shape[1]
     top_count = ids_ref.shape[0]
     cols = width // PARTS
-    band_rows = rows // BANDS
     half = taps_count // 2
     edge = (gated.shape[0] - block) // 2
     view = rows + 2 * edge
@@ -43,6 +45,9 @@
     mate = t + 1 - 2 * core
     chunks = chans // rows
     base = 2 * chunks
+
+    def band(k):
+        return pl.ds(BANDS[k] * rows // BANDS[-1], (BANDS[k + 1] - BANDS[k]) * rows // BANDS[-1])
 
     def col(c):
         return pl.ds(c * cols, cols)
@@ -58,7 +63,7 @@
                 (ids_hbm, ids_ref),
                 (share_hbm, share_ref),
                 (gain_hbm, gain_ref),
-                (latent_hbm, out_ref),
+                (latent_hbm, kept),
             )
         )
     ]
@@ -69,7 +74,7 @@
         pltpu.make_async_copy(
             weight_hbm.at[pl.ds(b * rows, rows), col(c)],
             inc.at[core * chunks + b, c],
-            point_sem.at[b, c],
+            point_sem.at[0],
         )
         for b in range(chunks)
         for c in range(PARTS)
@@ -127,9 +132,8 @@
     def _():
         halo_copy(0).start()
 
-    for load in point_loads:
-        load.wait()
     own_rows = pl.ds(core * chunks, chunks)
+    pltpu.make_async_copy(inc.at[own_rows], inc.at[own_rows], point_sem.at[0]).wait()
     mate_copy = pltpu.make_async_remote_copy(
         src_ref=inc.at[own_rows], dst_ref=inc.at[own_rows],
         send_sem=mate_send.at[0], recv_sem=mate_recv.at[0],
@@ -184,7 +188,7 @@
     def stat_copy(p):
         return pltpu.make_async_remote_copy(
             src_ref=stats.at[t], dst_ref=stats.at[t],
-            send_sem=stat_send.at[p], recv_sem=stat_recv.at[t],
+            send_sem=stat_send.at[0], recv_sem=stat_recv.at[0],
             device_id={"tp": lax.rem(t + p, tp)}, device_id_type=MESH,
         )
 
@@ -207,9 +211,8 @@
         tabs[z, pl.ds(k, 1)] = ids[k : k + 1] * cap + count
         tabs[z, pl.ds(top_count + k, 1)] = share_ref[pl.ds(k, 1)]
 
-    for p in range(1, tp):
-        other = lax.rem(t + p, tp)
-        pltpu.make_async_copy(stats.at[other], stats.at[other], stat_recv.at[other]).wait()
+    others = stats.at[pl.ds(0, tp - 1)]
+    pltpu.make_async_copy(others, others, stat_recv.at[0]).wait()
 
     def activate(s):
         both = stats[0, s]
@@ -249,10 +252,10 @@
         return jnp.dot(left, right, preferred_element_type=jnp.float32)
 
     def part_copy(i, k):
-        piece = pl.ds(k * band_rows, band_rows)
+        piece = band(k)
         return pltpu.make_async_remote_copy(
             src_ref=psend.at[i - 1, :, piece], dst_ref=inc.at[base + i - 1, :, piece],
-            send_sem=part_send.at[i - 1, k], recv_sem=part_recv.at[i - 1, k],
+            send_sem=part_send.at[i - 1], recv_sem=part_recv.at[i - 1, k],
             device_id={"tp": 2 * lax.rem(quad + i, q_count) + core}, device_id_type=MESH,
         )
 
@@ -265,14 +268,14 @@
             else:
                 acc[c] = product(i, c)
         if i:
-            for k in range(BANDS):
+            for k in range(len(BANDS) - 1):
                 part_copy(i, k).start()
 
     def token_copy(zs, k, side):
-        piece = pl.ds(k * band_rows, band_rows)
+        piece = band(k)
         return pltpu.make_async_remote_copy(
             src_ref=toks.at[zs, :, piece], dst_ref=toks.at[zs, :, piece],
-            send_sem=tok_send.at[side, zs, k], recv_sem=tok_recv.at[zs, k],
+            send_sem=tok_send.at[side, zs], recv_sem=tok_recv.at[zs, k],
             device_id={"sp": z + 1 if side else z - 1}, device_id_type=MESH,
         )
 
@@ -294,63 +297,76 @@
 
     each_side(z, lambda side: table_copy(z, side).start())
 
-    for k in range(BANDS):
-        piece = pl.ds(k * band_rows, band_rows)
+    for k in range(len(BANDS) - 1):
+        piece = band(k)
         for i in range(1, q_count):
             spot = inc.at[base + i - 1, :, piece]
             pltpu.make_async_copy(spot, spot, part_recv.at[i - 1, k]).wait()
-        square = jnp.zeros((band_rows, 1), jnp.float32)
+        square = jnp.zeros((piece.size, 1), jnp.float32)
         for c in range(PARTS):
-            total = acc[c, piece] + out_ref[piece, col(c)].astype(jnp.float32)
+            total = acc[c, piece] + kept[piece, col(c)].astype(jnp.float32)
             for i in range(1, q_count):
                 total = total + inc[base + i - 1, c, piece].astype(jnp.float32)
             after = total.astype(jnp.bfloat16)
-            out_ref[piece, col(c)] = after
+            kept[piece, col(c)] = after
             after = after.astype(jnp.float32)
             square = square + jnp.sum(after * after, axis=1, keepdims=True)
         norm = lax.rsqrt(square / width + 0.01)
         for c in range(PARTS):
-            after = out_ref[piece, col(c)].astype(jnp.float32)
+            after = kept[piece, col(c)].astype(jnp.float32)
             toks[z, c, piece] = (after * norm * gain_ref[:, col(c)]).astype(jnp.bfloat16)
         each_side(z, lambda side: token_copy(z, k, side).start())
 
 
-    def source(j):
+    upper = z > n - 1 - z
+    middle = (z > 0) & (z < n - 1)
+
+    def arrival(j):
         low = jnp.minimum(z, n - 1 - z)
-        near = jnp.where(j % 2 == 1, z - (j + 1) // 2, z + j // 2)
-        far = jnp.where(z > n - 1 - z, z - (j - low), z + (j - low))
-        return jnp.where(j <= 2 * low, near, far)
+        out = jnp.where(j <= 2 * low, (j + 1) // 2, j - low)
+        down = jnp.where(j <= 2 * low, (j % 2 == 1) == upper, upper)
+        return jnp.where(down, z - out, z + out)
+
+    def source(i):
+        mine = jnp.where(middle, 0, n - 1)
+        return jnp.where(i == mine, z, arrival(jnp.where(middle, i, i + 1)))
 
     def span(index):
         return pl.ds(pl.multiple_of(index * cap, 16), cap)
 
-    def exchange(j, c, to_ref, zs, ss, rs):
-        page = lax.rem(j, 2)
+    def exchange(j, c, to_ref, ss, rs):
+        page = lax.rem(j, PAGES)
         for p in range(1, tp):
             other = lax.rem(t + p, tp)
             pltpu.make_async_remote_copy(
                 src_ref=comp.at[page, c, span(other)],
-                dst_ref=to_ref.at[zs, c, span(t)],
-                send_sem=ss.at[zs, c],
-                recv_sem=rs.at[zs, c],
+                dst_ref=to_ref.at[page, c, span(t)],
+                send_sem=ss.at[page],
+                recv_sem=rs.at[page, c],
                 device_id={"tp": other},
                 device_id_type=MESH,
             ).start()
-        to_ref[zs, c, span(t)] = comp[page, c, span(t)]
-
-    def wait_pieces(ref, zs, c, ss, rs):
-        part = ref.at[zs, c, pl.ds(0, (tp - 1) * cap)]
-        pltpu.make_async_copy(part, part, rs.at[zs, c]).wait()
-        pltpu.make_async_copy(part, part, ss.at[zs, c]).wait()
-
-    def sum_copy(zs, c, side):
+        to_ref[page, c, span(t)] = comp[page, c, span(t)]
+
+    def wait_pieces(ref, page, c, rs):
+        part = ref.at[page, c, pl.ds(0, (tp - 1) * cap)]
+        pltpu.make_async_copy(part, part, rs.at[page, c]).wait()
+
+    def wait_sent(page, ss):
+        part = comp.at[page, :, pl.ds(0, (tp - 1) * cap)]
+        pltpu.make_async_copy(part, part, ss.at[page]).wait()
+
+    def piece_of(h):
+        return pl.ds(h * (rows // SPLIT), rows // SPLIT)
+
+    def sum_copy(zs, c, h, side):
         target = z + 1 if side else z - 1
         slot = jnp.where(target == zs, n, zs) if side else zs
         return pltpu.make_async_remote_copy(
-            src_ref=toks.at[zs, c],
-            dst_ref=inc.at[slot, c],
-            send_sem=sum_send.at[zs, c],
-            recv_sem=sum_recv.at[slot, c],
+            src_ref=toks.at[zs, c, piece_of(h)],
+            dst_ref=inc.at[slot, c, piece_of(h)],
+            send_sem=sum_send.at[zs],
+            recv_sem=sum_recv.at[slot, c, h],
             device_id={"sp": target},
             device_id_type=MESH,
         )
@@ -365,17 +381,22 @@
         return ((zs < z) & (z < n - 1)) | ((zs > z) & (z > 0))
 
     def arrive(zs, k):
-        spot = toks.at[zs, :, pl.ds(k * band_rows, band_rows)]
+        spot = toks.at[zs, :, band(k)]
         pltpu.make_async_copy(spot, spot, tok_recv.at[zs, k]).wait()
 
+    def wait_passed(zs, side):
+        table_copy(zs, side).wait_send()
+        pltpu.make_async_copy(toks.at[zs], toks.at[zs], tok_send.at[side, zs]).wait()
+
     def hand_on(j):
-        zs = source(jnp.minimum(j, n - 1))
-
-        @pl.when((j < n) & passes_on(zs))
-        def _():
+        zs = arrival(jnp.minimum(j + 1, n - 1))
+
+        @pl.when((j < n - 1) & passes_on(zs))
+        def _():
+            each_side(zs, lambda side: wait_passed(jnp.where(zs < z, zs + 1, zs - 1), side))
             pltpu.make_async_copy(tabs.at[zs], tabs.at[zs], tab_recv.at[zs]).wait()
             each_side(zs, lambda side: table_copy(zs, side).start())
-            for k in range(BANDS):
+            for k in range(len(BANDS) - 1):
                 arrive(zs, k)
                 each_side(zs, lambda side: token_copy(zs, k, side).start())
 
@@ -385,20 +406,20 @@
         @pl.when((zs != z) & jnp.logical_not(passes_on(zs)))
         def _():
             pltpu.make_async_copy(tabs.at[zs], tabs.at[zs], tab_recv.at[zs]).wait()
-            for k in range(BANDS):
+            for k in range(len(BANDS) - 1):
                 arrive(zs, k)
 
         first, second, _ = names(zs)
         pick = jnp.where(first | second, 1.0, 0.0).astype(jnp.bfloat16)
-        page = lax.rem(j, 2)
+        page = lax.rem(j, PAGES)
         for c in range(PARTS):
             comp[page, c] = jnp.dot(
                 pick, toks[zs, c], preferred_element_type=jnp.float32
             ).astype(jnp.bfloat16)
-            exchange(j, c, arr, zs, piece_send, piece_recv)
+            exchange(j, c, arr, piece_send, piece_recv)
 
     def run(j):
-        zs = source(j)
+        page = lax.rem(j, PAGES)
 
         @pl.when(j == 0)
         def _():
@@ -407,11 +428,11 @@
 
         step = 256
         for c in range(PARTS):
-            wait_pieces(arr, zs, c, piece_send, piece_recv)
+            wait_pieces(arr, page, c, piece_recv)
             for f in range(0, hidden_width, step):
                 for to, weights in ((ga, wg), (ua, wu)):
                     value = jnp.dot(
-                        arr[zs, c], weights[col(c), f : f + step],
+                        arr[page, c], weights[col(c), f : f + step],
                         preferred_element_type=jnp.float32,
                     )
                     if c:
@@ -421,15 +442,16 @@
                 if c == PARTS - 1:
                     gate = ga[:, f : f + step]
                     hid[:, f : f + step] = (jax.nn.silu(gate) * value).astype(jnp.bfloat16)
-        page = lax.rem(j, 2)
+        wait_sent(page, piece_send)
         for c in range(PARTS):
             comp[page, c] = jnp.dot(
                 hid[...], wd[:, col(c)], preferred_element_type=jnp.float32
             ).astype(jnp.bfloat16)
-            exchange(j, c, back, zs, back_send, back_recv)
-
-    def merge(j):
+            exchange(j, c, back, back_send, back_recv)
+
+    def merge(j, after_part):
         zs = source(j)
+        page = lax.rem(j, PAGES)
         first, second, table = names(zs)
         share = jnp.where(first, table[2:3, :], 0.0) + jnp.where(second, table[3:4, :], 0.0)
         share = share.T
@@ -437,15 +459,15 @@
         rest = (share - high.astype(jnp.float32)).astype(jnp.bfloat16)
 
         def sent(side):
-            table_copy(zs, side).wait_send()
-            for k in range(BANDS):
-                token_copy(zs, k, side).wait_send()
+            @pl.when(zs == (0 if side else n - 1))
+            def _():
+                wait_passed(zs, side)
 
         each_side(zs, sent)
         for c in range(PARTS):
-            wait_pieces(back, zs, c, back_send, back_recv)
-            value = jnp.dot(high, back[zs, c], preferred_element_type=jnp.float32) + jnp.dot(
-                rest, back[zs, c], preferred_element_type=jnp.float32
+            wait_pieces(back, page, c, back_recv)
+            value = jnp.dot(high, back[page, c], preferred_element_type=jnp.float32) + jnp.dot(
+                rest, back[page, c], preferred_element_type=jnp.float32
             )
 
             @pl.when(zs == z)
@@ -456,107 +478,120 @@
             def _():
                 toks[zs, c] = value.astype(jnp.bfloat16)
 
-            @pl.when((zs < z) & (z == n - 1))
+            after_part(zs, c)
+        wait_sent(page, back_send)
+
+    def send_sums(zs, c):
+        for side in range(2):
+            @pl.when((zs > z) & (z == 0) if side else (zs < z) & (z == n - 1))
             def _():
-                sum_copy(zs, c, 0).start()
-
-            @pl.when((zs > z) & (z == 0))
-            def _():
-                sum_copy(zs, c, 1).start()
-
-    upper = z > n - 1 - z
-
-    def relay(turn):
-        def pass_sum(zs, side, c):
-            spot = inc.at[zs, c]
-            pltpu.make_async_copy(spot, spot, sum_recv.at[zs, c]).wait()
-            toks[zs, c] = (
-                toks[zs, c].astype(jnp.float32) + inc[zs, c].astype(jnp.float32)
+                for h in range(SPLIT):
+                    sum_copy(zs, c, h, side).start()
+
+    def relay(turn, p, side):
+        zs = turn if side else n - 1 - turn
+        c, h = p // SPLIT, p % SPLIT
+
+        @pl.when((z > 0) & (z < turn) if side else (z < n - 1) & (z > n - 1 - turn))
+        def _():
+            spot = inc.at[zs, c, piece_of(h)]
+            pltpu.make_async_copy(spot, spot, sum_recv.at[zs, c, h]).wait()
+            toks[zs, c, piece_of(h)] = (
+                toks[zs, c, piece_of(h)].astype(jnp.float32)
+                + inc[zs, c, piece_of(h)].astype(jnp.float32)
             ).astype(jnp.bfloat16)
-            sum_copy(zs, c, side).start()
-
-        def go_up(c):
-            @pl.when((z > 0) & (z < turn))
-            def _():
-                pass_sum(turn, 1, c)
-
-        def go_down(c):
-            @pl.when((z < n - 1) & (z > n - 1 - turn))
-            def _():
-                pass_sum(n - 1 - turn, 0, c)
-
-        for c in range(PARTS):
-            @pl.when(upper)
-            def _():
-                go_down(c)
-
-            go_up(c)
-
-            @pl.when(jnp.logical_not(upper))
-            def _():
-                go_down(c)
+            sum_copy(zs, c, h, side).start()
+
+    def relays(turn, start, stop):
+        def both(side):
+            for p in range(start, stop):
+                if p < PARTS * SPLIT:
+                    relay(turn, p, side)
+                if p >= LAG:
+                    relay(turn, p - LAG, 1 - side)
+
+        @pl.when((turn > 0) & upper)
+        def _():
+            both(0)
+
+        @pl.when((turn > 0) & jnp.logical_not(upper))
+        def _():
+            both(1)
+
+    def merge_and_relay(j):
+        merge(j, lambda zs, c: relays(j, c * SPLIT, (c + 1) * SPLIT))
+        relays(j, PARTS * SPLIT, PARTS * SPLIT + LAG)
 
     def body(j, carry):
-        @pl.when(j == 1)
-        def _():
-            hand_on(j)
-
-        @pl.when(j > 0)
-        def _():
-            hand_on(j + 1)
+        hand_on(j + 1)
+        ahead = jnp.where(middle, j + 1, j)
+
+        @pl.when(ahead < n)
+        def _():
+            take(ahead)
+
+        @pl.when((j > 0) & jnp.logical_not(middle))
+        def _():
+            merge(j - 1, send_sums)
 
         @pl.when(j < n)
         def _():
-            take(j)
-
-        @pl.when((j > 0) & (j <= n))
-        def _():
-            merge(j - 1)
-
-        @pl.when(j < n)
-        def _():
             run(j)
 
-        @pl.when(j > 2)
-        def _():
-            relay(j - 2)
+        @pl.when((j > 0) & middle)
+        def _():
+            merge_and_relay(j - 1)
 
         return carry
 
-    lax.fori_loop(0, n + 2, body, 0)
+    @pl.when(middle)
+    def _():
+        take(0)
+        hand_on(0)
+
+    lax.fori_loop(0, n + 1, body, 0)
+
+    def final(c, h):
+        piece = piece_of(h)
+
+        @pl.when(z < n - 1)
+        def _():
+            spot = inc.at[z, c, piece]
+            pltpu.make_async_copy(spot, spot, sum_recv.at[z, c, h]).wait()
+            acc[c, piece] = acc[c, piece] + inc[z, c, piece].astype(jnp.float32)
+
+        @pl.when(z > 0)
+        def _():
+            spot = inc.at[n, c, piece]
+            pltpu.make_async_copy(spot, spot, sum_recv.at[n, c, h]).wait()
+            acc[c, piece] = acc[c, piece] + inc[n, c, piece].astype(jnp.float32)
+
+        kept[piece, col(c)] = (
+            kept[piece, col(c)].astype(jnp.float32) + acc[c, piece]
+        ).astype(jnp.bfloat16)
+        pltpu.make_async_copy(
+            kept.at[piece, col(c)], out_hbm.at[piece, col(c)], out_sem.at[0]
+        ).start()
 
     for c in range(PARTS):
-        @pl.when(z < n - 1)
-        def _():
-            spot = inc.at[z, c]
-            pltpu.make_async_copy(spot, spot, sum_recv.at[z, c]).wait()
-            acc[c] = acc[c] + inc[z, c].astype(jnp.float32)
-
-        @pl.when(z > 0)
-        def _():
-            spot = inc.at[n, c]
-            pltpu.make_async_copy(spot, spot, sum_recv.at[n, c]).wait()
-            acc[c] = acc[c] + inc[n, c].astype(jnp.float32)
-
-        out_ref[:, col(c)] = (out_ref[:, col(c)].astype(jnp.float32) + acc[c]).astype(jnp.bfloat16)
+        for h in range(SPLIT):
+            final(c, h)
 
     def drain(zs, carry):
         @pl.when(zs != z)
         def _():
-            for c in range(PARTS):
-                spot = toks.at[zs, c]
-                pltpu.make_async_copy(spot, spot, sum_send.at[zs, c]).wait()
+            pltpu.make_async_copy(toks.at[zs], toks.at[zs], sum_send.at[zs]).wait()
 
         return carry
 
     lax.fori_loop(0, n, drain, 0)
-    for p in range(1, tp):
-        stat_copy(p).wait_send()
+    pltpu.make_async_copy(kept, out_hbm, out_sem.at[0]).wait()
+    pltpu.make_async_copy(others, others, stat_send.at[0]).wait()
     for i in order:
         act_copy(i).wait_send()
         if i:
-            for k in range(BANDS):
-                part_copy(i, k).wait_send()
+            spot = psend.at[i - 1]
+            pltpu.make_async_copy(spot, spot, part_send.at[i - 1]).wait()
 
     @pl.when(z < n - 1)
     def _():
@@ -602,7 +637,7 @@
         functools.partial(layer_kernel, n, tp, taps_count, cap),
         out_shape=jax.ShapeDtypeStruct((rows, width), bf16),
         in_specs=[anywhere] * 12,
-        out_specs=pl.BlockSpec(memory_space=pltpu.VMEM),
+        out_specs=anywhere,
         scratch_shapes=[
             vmem((block, chans), bf16),
             vmem((block, chans), bf16),
@@ -611,6 +646,7 @@
             vmem((1, width), f32),
             vmem((top_count, rows), jnp.int32),
             vmem((top_count, rows), f32),
+            vmem((rows, width), bf16),
             vmem((block + 2 * edge, chans), bf16),
             vmem((rows + 2 * edge, chans), f32),
             vmem((tp, rows, chans), f32),
@@ -620,9 +656,9 @@
             vmem((q_count - 1, PARTS, rows, cols), bf16),
             vmem((n, PARTS, rows, cols), bf16),
             vmem((n, 8, rows), f32),
-            vmem((2, PARTS, slots, cols), bf16),
-            vmem((n, PARTS, slots, cols), bf16),
-            vmem((n, PARTS, slots, cols), bf16),
+            vmem((PAGES, PARTS, slots, cols), bf16),
+            vmem((PAGES, PARTS, slots, cols), bf16),
+            vmem((PAGES, PARTS, slots, cols), bf16),
             vmem((spots, PARTS, rows, cols), bf16),
             vmem((PARTS, rows, cols), f32),
             vmem((width, hidden_width), bf16),
@@ -632,28 +668,29 @@
             vmem((slots, hidden_width), f32),
             vmem((slots, hidden_width), bf16),
             dma((8,)),
-            dma((chans // rows, PARTS)),
+            dma((1,)),
             dma((3,)),
+            dma((1,)),
             dma((2,)),
             dma((2,)),
-            dma((tp,)),
-            dma((tp,)),
+            dma((1,)),
+            dma((1,)),
             dma((1,)),
             dma((1,)),
             dma((q_count,)),
             dma((q_count,)),
-            dma((q_count - 1, BANDS)),
-            dma((q_count - 1, BANDS)),
-            dma((2, n, BANDS)),
-            dma((n, BANDS)),
+            dma((q_count - 1,)),
+            dma((q_count - 1, len(BANDS) - 1)),
+            dma((2, n)),
+            dma((n, len(BANDS) - 1)),
             dma((2, n)),
             dma((n,)),
-            dma((n, PARTS)),
-            dma((n, PARTS)),
-            dma((n, PARTS)),
-            dma((n, PARTS)),
-            dma((n, PARTS)),
-            dma((n + 1, PARTS)),
+            dma((PAGES,)),
+            dma((PAGES, PARTS)),
+            dma((PAGES,)),
+            dma((PAGES, PARTS)),
+            dma((n,)),
+            dma((n + 1, PARTS, SPLIT)),
         ],
         compiler_params=pltpu.CompilerParams(
             collective_id=0, has_side_effects=True, vmem_limit_bytes=67043328

time: 122 us -> 97.6 us (0.80)
  Pallas kernels: 120 us -> 95.6 us
    pallas_call x1, Pallas kernels: 120 us -> 95.6 us  [shards(): pl.pallas_call(functools.partial(layer_kernel, n, tp, taps_count, cap), o...]
where the time goes in v2:
time: 97.6 us; the launch traced here: 97.5 us
  Pallas kernels  95.6 us (98%)
  local copies, waits for them, and re-layouts  1.88 us (2%)
    pallas_call x1, Pallas kernels, shards(): pl.pallas_call(functools.partial(layer_kernel, n, tp, taps_count, cap), o...  95.6 us

profile of v2, /device:TPU:0, one launch (start us, length us, event | category | flops | bytes accessed | tf_op | source)
XLA Modules:
  0.0 97.5 jit_solution(15545141367294412818)
XLA Ops:
  0.0 95.6 %layer.1 = bf16[128,2048]{1,0:T(8,128)(2,1)} custom-call(bf16[512,256]{1,0:T(8,128)(2,1)} %value_hbm.1, bf16[512,256]{1,0:T(8,128)(2,1)} %gate_hbm.1, f32[31,256]{1,0:T(8,128)} %taps_hbm.1, f32[1,256]{1,0:T(1,128)} %bitcast.5, bf16[256,2048]{1,0:T(8,128)(2,1)} %weight_hbm.1, bf16[128,2048]{1,0:T(8,128)(2,1)} %latent_hbm.1, f32[1,2048]{1,0:T(1,128)} %bitcast.4, ...), custom_call_target="tpu_custom_call" | custom-call | tf_op jit(solution)/shard_map/layer/pallas_call | solution.py:636
  95.6 1.9 %copy.14 = bf16[128,2048]{1,0:T(8,128)(2,1)} copy(bf16[128,2048]{1,0:T(8,128)(2,1)} %layer.1) | data formatting | bytes 1048576

commit v3 on v2

--- a/solution.py
+++ b/solution.py
@@ -22,23 +22,26 @@
     wg_hbm, wu_hbm, wd_hbm, out_hbm,
     value_ref, gate_ref, taps_ref, cgain_ref, gain_ref, ids_ref, share_ref,
     kept, gated, wide, mixed, stats, act_out, act_in, psend,
-    toks, tabs, comp, arr, back, inc, acc, wg, wu, wd, ga, ua, hid,
+    toks, tabs, comp, outs, arr, back, inc, acc, wg, wu, wd, ga, ua, hid,
     load_sem, point_sem, w_sem, out_sem, halo_send, halo_recv, stat_send, stat_recv, mate_send, mate_recv,
     act_send, act_recv, part_send, part_recv,
     tok_send, tok_recv, tab_send, tab_recv,
-    piece_send, piece_recv, back_send, back_recv, sum_send, sum_recv,
+    piece_send, piece_recv, back_send, back_recv, sum_send, sum_recv, turn_sem,
 ):
     z = lax.axis_index("sp")
     t = lax.axis_index("tp")
     block, chans = value_ref.shape
     rows, width = kept.shape
     slots = tp * cap
+    groups = 2 if cap % 32 == 0 else 1
+    depth = cap // groups
+    group_rows = slots // groups
     hidden_width = wg.shape[1]
     top_count = ids_ref.shape[0]
     cols = width // PARTS
     half = taps_count // 2
     edge = (gated.shape[0] - block) // 2
-    view = rows + 2 * edge
+    view = rows // 2 + 2 * edge
     q_count = tp // 2
     core = lax.rem(t, 2)
     quad = t // 2
@@ -145,55 +148,65 @@
         pltpu.make_async_copy(a, b, w_sem.at[i])
         for i, (a, b) in enumerate(((wg_hbm.at[0], wg), (wu_hbm.at[0], wu), (wd_hbm.at[0], wd)))
     ]
+    for load in loads[2:]:
+        load.wait()
+
+    tile = rows // 2
+
+    def convolve(s, r):
+        start = pl.multiple_of(s * rows + r, 16)
+        wide[0] = gated[pl.ds(start, view)].astype(jnp.float32)
+        for b in range(1, 8):
+            wide[b, pl.ds(0, view - 8)] = wide[0, pl.ds(b, view - 8)]
+        value = jnp.zeros((tile, chans), jnp.float32)
+        for i in range(taps_count):
+            a, b = divmod(edge - half + i, 8)
+            value = value + taps_ref[pl.ds(i, 1)] * wide[b, pl.ds(8 * a, tile)]
+        mixed[s, pl.ds(pl.multiple_of(r, 16), tile)] = value
+
+    def measure(s):
+        value = mixed[s]
+        for k, summed in enumerate((value, value * value)):
+            line = jnp.broadcast_to(jnp.sum(summed, axis=1, keepdims=True), (rows, rows)).T
+            stats[t, s, pl.ds(k, 1)] = line[0:1]
+        for p in range(1, tp):
+            pltpu.make_async_remote_copy(
+                src_ref=stats.at[t, s], dst_ref=stats.at[t, s],
+                send_sem=stat_send.at[0], recv_sem=stat_recv.at[s],
+                device_id={"tp": lax.rem(t + p, tp)}, device_id_type=MESH,
+            ).start()
+
+    def inner(i, carry):
+        s = jnp.where(quad == 0, tp - 2 - i, i + 1)
+        convolve(s, 0)
+        convolve(s, tile)
+        measure(s)
+        return carry
+
+    def near_edge(i, carry):
+        convolve(i * (tp - 1), (1 - i) * tile)
+        return carry
+
+    def at_edge(i, carry):
+        side = jnp.where(quad == 0, 1 - i, i)
+        convolve(side * (tp - 1), side * tile)
+        measure(side * (tp - 1))
+        return carry
+
+    lax.fori_loop(0, tp - 2, inner, 0)
+    lax.fori_loop(0, 2, near_edge, 0)
+
+    @pl.when(z > 0)
+    def _():
+        halo_copy(1).wait_recv()
+
+    @pl.when(z < n - 1)
+    def _():
+        halo_copy(0).wait_recv()
+
+    lax.fori_loop(0, 2, at_edge, 0)
     for load in expert_loads:
         load.start()
-    for load in loads[2:]:
-        load.wait()
-
-    def convolve(s):
-        wide[...] = gated[pl.ds(pl.multiple_of(s * rows, 16), view)].astype(jnp.float32)
-        tile = 64
-        sums, squares = [], []
-        for r in range(0, rows, tile):
-            value = jnp.zeros((tile, chans), jnp.float32)
-            for i in range(taps_count):
-                value = value + taps_ref[pl.ds(i, 1)] * wide[pl.ds(edge - half + i + r, tile)]
-            mixed[s, pl.ds(r, tile)] = value
-            sums.append(jnp.sum(value, axis=1, keepdims=True))
-            squares.append(jnp.sum(value * value, axis=1, keepdims=True))
-        for k, parts in enumerate((sums, squares)):
-            line = jnp.broadcast_to(jnp.concatenate(parts, axis=0), (rows, rows)).T
-            stats[t, s, pl.ds(k, 1)] = line[0:1]
-
-    def inner(i, carry):
-        convolve(i + 1)
-        return carry
-
-    lax.fori_loop(0, tp - 2, inner, 0)
-
-    @pl.when(z > 0)
-    def _():
-        halo_copy(1).wait_recv()
-
-    @pl.when(z < n - 1)
-    def _():
-        halo_copy(0).wait_recv()
-
-    def outer(i, carry):
-        convolve(i * (tp - 1))
-        return carry
-
-    lax.fori_loop(0, 2, outer, 0)
-
-    def stat_copy(p):
-        return pltpu.make_async_remote_copy(
-            src_ref=stats.at[t], dst_ref=stats.at[t],
-            send_sem=stat_send.at[0], recv_sem=stat_recv.at[0],
-            device_id={"tp": lax.rem(t + p, tp)}, device_id_type=MESH,
-        )
-
-    for p in range(1, tp):
-        stat_copy(p).start()
 
     ids = ids_ref[...].astype(jnp.float32)
     across = [jnp.broadcast_to(ids[k : k + 1], (rows, rows)) for k in range(top_count)]
@@ -211,10 +224,9 @@
         tabs[z, pl.ds(k, 1)] = ids[k : k + 1] * cap + count
         tabs[z, pl.ds(top_count + k, 1)] = share_ref[pl.ds(k, 1)]
 
-    others = stats.at[pl.ds(0, tp - 1)]
-    pltpu.make_async_copy(others, others, stat_recv.at[0]).wait()
-
-    def activate(s):
+    def activate_block(s):
+        others = stats.at[pl.ds(0, tp - 1), s]
+        pltpu.make_async_copy(others, others, stat_recv.at[s]).wait()
         both = stats[0, s]
         for p in range(1, tp):
             both = both + stats[p, s]
@@ -226,50 +238,51 @@
         value = (mixed[s] - center) * scale * cgain_ref[...]
         return jax.nn.silu(value).astype(jnp.bfloat16)
 
-    def act_copy(i):
-        spot = lax.rem(quad + i, q_count)
+    def spot_of(e, which):
+        return jnp.where(which == 0, (e + 1) % q_count, e)
+
+    def act_copy(spot):
         return pltpu.make_async_remote_copy(
             src_ref=act_out.at[spot], dst_ref=act_in.at[spot, core],
-            send_sem=act_send.at[i], recv_sem=act_recv.at[spot],
+            send_sem=act_send.at[spot], recv_sem=act_recv.at[spot],
             device_id={"tp": mate}, device_id_type=MESH,
         )
 
-    order = list(range(1, q_count)) + [0]
-    for i in order:
-        spot = lax.rem(quad + i, q_count)
-        act_out[spot] = activate(2 * spot + 1 - core)
-        act_copy(i).start()
-    for i in order:
-        spot = lax.rem(quad + i, q_count)
-        act_in[spot, core] = activate(2 * spot + core)
-
-    mate_copy.wait()
-
-    def product(i, c):
-        spot = lax.rem(quad + i, q_count)
+    def product(spot, c):
         left = jnp.concatenate([act_in[spot, 0], act_in[spot, 1]], axis=1)
         right = inc[pl.ds(0, base), c].reshape(base * rows, cols)
         return jnp.dot(left, right, preferred_element_type=jnp.float32)
 
-    def part_copy(i, k):
+    def part_copy(spot, k):
+        i = lax.rem(spot - quad + q_count, q_count) - 1
         piece = band(k)
         return pltpu.make_async_remote_copy(
-            src_ref=psend.at[i - 1, :, piece], dst_ref=inc.at[base + i - 1, :, piece],
-            send_sem=part_send.at[i - 1], recv_sem=part_recv.at[i - 1, k],
-            device_id={"tp": 2 * lax.rem(quad + i, q_count) + core}, device_id_type=MESH,
-        )
-
-    for i in order:
-        spot = lax.rem(quad + i, q_count)
-        pltpu.make_async_copy(act_out.at[spot], act_out.at[spot], act_recv.at[spot]).wait()
-        for c in range(PARTS):
-            if i:
-                psend[i - 1, c] = product(i, c).astype(jnp.bfloat16)
-            else:
-                acc[c] = product(i, c)
-        if i:
+            src_ref=psend.at[i, :, piece], dst_ref=inc.at[base + i, :, piece],
+            send_sem=part_send.at[i], recv_sem=part_recv.at[i, k],
+            device_id={"tp": 2 * spot + core}, device_id_type=MESH,
+        )
+
+    for e in range(q_count):
+        theirs, ours = spot_of(e, 1 - core), spot_of(e, core)
+        act_out[theirs] = activate_block(2 * theirs + 1 - core)
+        act_copy(theirs).start()
+        act_in[ours, core] = activate_block(2 * ours + core)
+        if e == 0:
+            mate_copy.wait()
+        pltpu.make_async_copy(act_out.at[ours], act_out.at[ours], act_recv.at[ours]).wait()
+
+        @pl.when(ours != quad)
+        def _():
+            i = lax.rem(ours - quad + q_count, q_count) - 1
+            for c in range(PARTS):
+                psend[i, c] = product(ours, c).astype(jnp.bfloat16)
             for k in range(len(BANDS) - 1):
-                part_copy(i, k).start()
+                part_copy(ours, k).start()
+
+        @pl.when(ours == quad)
+        def _():
+            for c in range(PARTS):
+                acc[c] = product(ours, c)
 
     def token_copy(zs, k, side):
         piece = band(k)
@@ -331,30 +344,34 @@
         mine = jnp.where(middle, 0, n - 1)
         return jnp.where(i == mine, z, arrival(jnp.where(middle, i, i + 1)))
 
-    def span(index):
-        return pl.ds(pl.multiple_of(index * cap, 16), cap)
-
-    def exchange(j, c, to_ref, ss, rs):
+    def span(g, index):
+        return pl.ds(pl.multiple_of(g * group_rows + index * depth, 16), depth)
+
+    def group(g):
+        return pl.ds(g * group_rows, group_rows)
+
+    def exchange(j, g, c, from_ref, to_ref, ss, rs):
         page = lax.rem(j, PAGES)
+        side = lax.rem(j, 2)
         for p in range(1, tp):
             other = lax.rem(t + p, tp)
             pltpu.make_async_remote_copy(
-                src_ref=comp.at[page, c, span(other)],
-                dst_ref=to_ref.at[page, c, span(t)],
-                send_sem=ss.at[page],
-                recv_sem=rs.at[page, c],
+                src_ref=from_ref.at[side, c, span(g, other)],
+                dst_ref=to_ref.at[page, c, span(g, t)],
+                send_sem=ss.at[side],
+                recv_sem=rs.at[page, g, c],
                 device_id={"tp": other},
                 device_id_type=MESH,
             ).start()
-        to_ref[page, c, span(t)] = comp[page, c, span(t)]
-
-    def wait_pieces(ref, page, c, rs):
-        part = ref.at[page, c, pl.ds(0, (tp - 1) * cap)]
-        pltpu.make_async_copy(part, part, rs.at[page, c]).wait()
-
-    def wait_sent(page, ss):
-        part = comp.at[page, :, pl.ds(0, (tp - 1) * cap)]
-        pltpu.make_async_copy(part, part, ss.at[page]).wait()
+        to_ref[page, c, span(g, t)] = from_ref[side, c, span(g, t)]
+
+    def wait_pieces(ref, page, g, c, rs):
+        part = ref.at[page, c, pl.ds(0, (tp - 1) * depth)]
+        pltpu.make_async_copy(part, part, rs.at[page, g, c]).wait()
+
+    def wait_sent(j, from_ref, ss):
+        part = from_ref.at[lax.rem(j, 2), :, pl.ds(0, (tp - 1) * cap)]
+        pltpu.make_async_copy(part, part, ss.at[lax.rem(j, 2)]).wait()
 
     def piece_of(h):
         return pl.ds(h * (rows // SPLIT), rows // SPLIT)
@@ -374,7 +391,11 @@
     def names(zs):
         table = tabs[zs]
         start = (z * slots).astype(jnp.float32)
-        place = lax.broadcasted_iota(jnp.int32, (slots, rows), 0).astype(jnp.float32) + start
+        row = lax.broadcasted_iota(jnp.int32, (slots, rows), 0)
+        place = (
+            lax.rem(row, group_rows) // depth * cap + row // group_rows * depth + lax.rem(row, depth)
+        )
+        place = place.astype(jnp.float32) + start
         return place == table[0:1, :], place == table[1:2, :], table
 
     def passes_on(zs):
@@ -393,7 +414,12 @@
 
         @pl.when((j < n - 1) & passes_on(zs))
         def _():
-            each_side(zs, lambda side: wait_passed(jnp.where(zs < z, zs + 1, zs - 1), side))
+            previous = jnp.where(zs < z, zs + 1, zs - 1)
+
+            @pl.when(previous != z)
+            def _():
+                each_side(zs, lambda side: wait_passed(previous, side))
+
             pltpu.make_async_copy(tabs.at[zs], tabs.at[zs], tab_recv.at[zs]).wait()
             each_side(zs, lambda side: table_copy(zs, side).start())
             for k in range(len(BANDS) - 1):
@@ -411,15 +437,19 @@
 
         first, second, _ = names(zs)
         pick = jnp.where(first | second, 1.0, 0.0).astype(jnp.bfloat16)
-        page = lax.rem(j, PAGES)
+        side = lax.rem(j, 2)
         for c in range(PARTS):
-            comp[page, c] = jnp.dot(
+            comp[side, c] = jnp.dot(
                 pick, toks[zs, c], preferred_element_type=jnp.float32
             ).astype(jnp.bfloat16)
-            exchange(j, c, arr, piece_send, piece_recv)
-
-    def run(j):
+            exchange(j, 0, c, comp, arr, piece_send, piece_recv)
+        for g in range(1, groups):
+            for c in range(PARTS):
+                exchange(j, g, c, comp, arr, piece_send, piece_recv)
+
+    def run(j, after_group):
         page = lax.rem(j, PAGES)
+        side = lax.rem(j, 2)
 
         @pl.when(j == 0)
         def _():
@@ -427,27 +457,29 @@
                 load.wait()
 
         step = 256
-        for c in range(PARTS):
-            wait_pieces(arr, page, c, piece_recv)
-            for f in range(0, hidden_width, step):
-                for to, weights in ((ga, wg), (ua, wu)):
-                    value = jnp.dot(
-                        arr[page, c], weights[col(c), f : f + step],
-                        preferred_element_type=jnp.float32,
-                    )
-                    if c:
-                        value = value + to[:, f : f + step]
-                    if c < PARTS - 1 or to is ga:
-                        to[:, f : f + step] = value
-                if c == PARTS - 1:
-                    gate = ga[:, f : f + step]
-                    hid[:, f : f + step] = (jax.nn.silu(gate) * value).astype(jnp.bfloat16)
-        wait_sent(page, piece_send)
-        for c in range(PARTS):
-            comp[page, c] = jnp.dot(
-                hid[...], wd[:, col(c)], preferred_element_type=jnp.float32
-            ).astype(jnp.bfloat16)
-            exchange(j, c, back, back_send, back_recv)
+        for g in range(groups):
+            for c in range(PARTS):
+                wait_pieces(arr, page, g, c, piece_recv)
+                for f in range(0, hidden_width, step):
+                    for to, weights in ((ga, wg), (ua, wu)):
+                        value = jnp.dot(
+                            arr[page, c, group(g)], weights[col(c), f : f + step],
+                            preferred_element_type=jnp.float32,
+                        )
+                        if c:
+                            value = value + to[:, f : f + step]
+                        if c < PARTS - 1 or to is ga:
+                            to[:, f : f + step] = value
+                    if c == PARTS - 1:
+                        gate = ga[:, f : f + step]
+                        hid[:, f : f + step] = (jax.nn.silu(gate) * value).astype(jnp.bfloat16)
+            for c in range(PARTS):
+                outs[side, c, group(g)] = jnp.dot(
+                    hid[...], wd[:, col(c)], preferred_element_type=jnp.float32
+                ).astype(jnp.bfloat16)
+                exchange(j, g, c, outs, back, back_send, back_recv)
+            after_group(g)
+        wait_sent(j, comp, piece_send)
 
     def merge(j, after_part):
         zs = source(j)
@@ -459,13 +491,14 @@
         rest = (share - high.astype(jnp.float32)).astype(jnp.bfloat16)
 
         def sent(side):
-            @pl.when(zs == (0 if side else n - 1))
+            @pl.when((zs == (0 if side else n - 1)) & ((zs != z) | jnp.logical_not(middle)))
             def _():
                 wait_passed(zs, side)
 
         each_side(zs, sent)
         for c in range(PARTS):
-            wait_pieces(back, page, c, back_recv)
+            for g in range(groups):
+                wait_pieces(back, page, g, c, back_recv)
             value = jnp.dot(high, back[page, c], preferred_element_type=jnp.float32) + jnp.dot(
                 rest, back[page, c], preferred_element_type=jnp.float32
             )
@@ -479,7 +512,7 @@
                 toks[zs, c] = value.astype(jnp.bfloat16)
 
             after_part(zs, c)
-        wait_sent(page, back_send)
+        wait_sent(j, outs, back_send)
 
     def send_sums(zs, c):
         for side in range(2):
@@ -518,25 +551,66 @@
         def _():
             both(1)
 
+    def merged(zs, j):
+        out = jnp.abs(zs - z)
+        low = jnp.minimum(z, n - 1 - z)
+        near = jnp.where((zs < z) == upper, 2 * out - 1, 2 * out)
+        return jnp.where(out <= low, near, out + low) < j
+
+    def is_early(turn):
+        up = (z >= turn) | merged(turn, turn)
+        down = (z <= n - 1 - turn) | merged(n - 1 - turn, turn)
+        return middle & (turn > 0) & up & down
+
+    pieces = PARTS * SPLIT
+    early_stops = (pieces // 4, pieces // 2 + 1, pieces + LAG)
+
+    def early_relays(turn, stop):
+        start = (0,) + early_stops
+        start = start[start.index(stop) - 1]
+
+        @pl.when(is_early(turn))
+        def _():
+            relays(turn, start, stop)
+
     def merge_and_relay(j):
-        merge(j, lambda zs, c: relays(j, c * SPLIT, (c + 1) * SPLIT))
-        relays(j, PARTS * SPLIT, PARTS * SPLIT + LAG)
+        late = jnp.logical_not(is_early(j))
+
+        def after(zs, c):
+            @pl.when(late)
+            def _():
+                relays(j, c * SPLIT, (c + 1) * SPLIT)
+
+        merge(j, after)
+
+        @pl.when(late)
+        def _():
+            relays(j, pieces, pieces + LAG)
 
     def body(j, carry):
-        hand_on(j + 1)
         ahead = jnp.where(middle, j + 1, j)
 
+        @pl.when((j == 1) & jnp.logical_not(middle))
+        def _():
+            merge(j - 1, send_sums)
+
         @pl.when(ahead < n)
         def _():
             take(ahead)
 
-        @pl.when((j > 0) & jnp.logical_not(middle))
+        @pl.when((j > 1) & jnp.logical_not(middle))
         def _():
             merge(j - 1, send_sums)
 
         @pl.when(j < n)
         def _():
-            run(j)
+            early_relays(j - 1, early_stops[0])
+            run(j, lambda g: early_relays(j - 1, early_stops[min(g + 1, 1)]) if g == 0 else None)
+            early_relays(j - 1, early_stops[2])
+
+        @pl.when(j > 0)
+        def _():
+            hand_on(j + 1)
 
         @pl.when((j > 0) & middle)
         def _():
@@ -547,7 +621,11 @@
     @pl.when(middle)
     def _():
         take(0)
+        each_side(z, lambda side: wait_passed(z, side))
+        pl.semaphore_signal(turn_sem, inc=1, device_id={"tp": mate}, device_id_type=MESH)
+        pl.semaphore_wait(turn_sem, 1)
         hand_on(0)
+        hand_on(1)
 
     lax.fori_loop(0, n + 1, body, 0)
 
@@ -586,12 +664,12 @@
 
     lax.fori_loop(0, n, drain, 0)
     pltpu.make_async_copy(kept, out_hbm, out_sem.at[0]).wait()
+    others = stats.at[pl.ds(0, tp - 1)]
     pltpu.make_async_copy(others, others, stat_send.at[0]).wait()
-    for i in order:
-        act_copy(i).wait_send()
-        if i:
-            spot = psend.at[i - 1]
-            pltpu.make_async_copy(spot, spot, part_send.at[i - 1]).wait()
+    for e in range(q_count):
+        act_copy(e).wait_send()
+    for i in range(q_count - 1):
+        pltpu.make_async_copy(psend.at[i], psend.at[i], part_send.at[i]).wait()
 
     @pl.when(z < n - 1)
     def _():
@@ -625,6 +703,7 @@
     taps_count = conv_taps.shape[0]
     hidden_width = gate_weight.shape[2]
     slots = tp * cap
+    groups = 2 if cap % 32 == 0 else 1
     cols = width // PARTS
     edge = -(-(taps_count // 2) // 16) * 16
     q_count = tp // 2
@@ -648,7 +727,7 @@
             vmem((top_count, rows), f32),
             vmem((rows, width), bf16),
             vmem((block + 2 * edge, chans), bf16),
-            vmem((rows + 2 * edge, chans), f32),
+            vmem((8, rows // 2 + 2 * edge, chans), f32),
             vmem((tp, rows, chans), f32),
             vmem((tp, tp, 8, rows), f32),
             vmem((q_count, rows, chans), bf16),
@@ -656,7 +735,8 @@
             vmem((q_count - 1, PARTS, rows, cols), bf16),
             vmem((n, PARTS, rows, cols), bf16),
             vmem((n, 8, rows), f32),
-            vmem((PAGES, PARTS, slots, cols), bf16),
+            vmem((2, PARTS, slots, cols), bf16),
+            vmem((2, PARTS, slots, cols), bf16),
             vmem((PAGES, PARTS, slots, cols), bf16),
             vmem((PAGES, PARTS, slots, cols), bf16),
             vmem((spots, PARTS, rows, cols), bf16),
@@ -664,9 +744,9 @@
             vmem((width, hidden_width), bf16),
             vmem((width, hidden_width), bf16),
             vmem((hidden_width, width), bf16),
-            vmem((slots, hidden_width), f32),
-            vmem((slots, hidden_width), f32),
-            vmem((slots, hidden_width), bf16),
+            vmem((slots // groups, hidden_width), f32),
+            vmem((slots // groups, hidden_width), f32),
+            vmem((slots // groups, hidden_width), bf16),
             dma((8,)),
             dma((1,)),
             dma((3,)),
@@ -674,7 +754,7 @@
             dma((2,)),
             dma((2,)),
             dma((1,)),
-            dma((1,)),
+            dma((tp,)),
             dma((1,)),
             dma((1,)),
             dma((q_count,)),
@@ -685,12 +765,13 @@
             dma((n, len(BANDS) - 1)),
             dma((2, n)),
             dma((n,)),
-            dma((PAGES,)),
-            dma((PAGES, PARTS)),
-            dma((PAGES,)),
-            dma((PAGES, PARTS)),
+            dma((2,)),
+            dma((PAGES, groups, PARTS)),
+            dma((2,)),
+            dma((PAGES, groups, PARTS)),
             dma((n,)),
             dma((n + 1, PARTS, SPLIT)),
+            pltpu.SemaphoreType.REGULAR,
         ],
         compiler_params=pltpu.CompilerParams(
             collective_id=0, has_side_effects=True, vmem_limit_bytes=67043328

time: 97.6 us -> 89.2 us (0.914)
  Pallas kernels: 95.6 us -> 87.1 us
    pallas_call x1, Pallas kernels: 95.6 us -> 87.1 us  [shards(): pl.pallas_call(functools.partial(layer_kernel, n, tp, taps_count, cap), o...]
where the time goes in v3:
time: 89.2 us; the launch traced here: 89 us
  Pallas kernels  87.1 us (98%)
  local copies, waits for them, and re-layouts  1.88 us (2%)
    pallas_call x1, Pallas kernels, shards(): pl.pallas_call(functools.partial(layer_kernel, n, tp, taps_count, cap), o...  87.1 us
    unnamed x1, local copies, waits for them, and re-layouts  1.88 us

profile of v3, /device:TPU:0, one launch (start us, length us, event | category | flops | bytes accessed | tf_op | source)
XLA Modules:
  0.0 89.0 jit_solution(7701589314062554584)
XLA Ops:
  0.0 87.1 %layer.1 = bf16[128,2048]{1,0:T(8,128)(2,1)} custom-call(bf16[512,256]{1,0:T(8,128)(2,1)} %value_hbm.1, bf16[512,256]{1,0:T(8,128)(2,1)} %gate_hbm.1, f32[31,256]{1,0:T(8,128)} %taps_hbm.1, f32[1,256]{1,0:T(1,128)} %bitcast.5, bf16[256,2048]{1,0:T(8,128)(2,1)} %weight_hbm.1, bf16[128,2048]{1,0:T(8,128)(2,1)} %latent_hbm.1, f32[1,2048]{1,0:T(1,128)} %bitcast.4, ...), custom_call_target="tpu_custom_call" | custom-call | tf_op jit(solution)/shard_map/layer/pallas_call | solution.py:715
  87.1 1.9 %copy.14 = bf16[128,2048]{1,0:T(8,128)(2,1)} copy(bf16[128,2048]{1,0:T(8,128)(2,1)} %layer.1) | data formatting | bytes 1048576

commit v4 on v3

--- a/solution.py
+++ b/solution.py
@@ -11,19 +11,19 @@
 MESH = pl.DeviceIdType.MESH
 PARTS = 4
 BANDS = (0, 1, 2, 3, 4, 5, 6, 7, 8)
-SPLIT = 2
-LAG = 3
+SPLIT = 4
+LAG = 5
 PAGES = 3
 
 
 def layer_kernel(
     n, tp, taps_count, cap,
     value_hbm, gate_hbm, taps_hbm, cgain_hbm, weight_hbm, latent_hbm, gain_hbm, ids_hbm, share_hbm,
-    wg_hbm, wu_hbm, wd_hbm, out_hbm,
+    wg_hbm, wu_hbm, wd_hbm, kept,
     value_ref, gate_ref, taps_ref, cgain_ref, gain_ref, ids_ref, share_ref,
-    kept, gated, wide, mixed, stats, act_out, act_in, psend,
+    gated, wide, mixed, stats, act_out, act_in, psend,
     toks, tabs, comp, outs, arr, back, inc, acc, wg, wu, wd, ga, ua, hid,
-    load_sem, point_sem, w_sem, out_sem, halo_send, halo_recv, stat_send, stat_recv, mate_send, mate_recv,
+    load_sem, point_sem, w_sem, halo_send, halo_recv, stat_send, stat_recv, mate_send, mate_recv,
     act_send, act_recv, part_send, part_recv,
     tok_send, tok_recv, tab_send, tab_recv,
     piece_send, piece_recv, back_send, back_recv, sum_send, sum_recv, turn_sem,
@@ -196,18 +196,6 @@
     lax.fori_loop(0, tp - 2, inner, 0)
     lax.fori_loop(0, 2, near_edge, 0)
 
-    @pl.when(z > 0)
-    def _():
-        halo_copy(1).wait_recv()
-
-    @pl.when(z < n - 1)
-    def _():
-        halo_copy(0).wait_recv()
-
-    lax.fori_loop(0, 2, at_edge, 0)
-    for load in expert_loads:
-        load.start()
-
     ids = ids_ref[...].astype(jnp.float32)
     across = [jnp.broadcast_to(ids[k : k + 1], (rows, rows)) for k in range(top_count)]
     down = [value.T for value in across]
@@ -223,6 +211,18 @@
             count = count + jnp.sum(jnp.where(same, 1.0, 0.0), axis=0, keepdims=True)
         tabs[z, pl.ds(k, 1)] = ids[k : k + 1] * cap + count
         tabs[z, pl.ds(top_count + k, 1)] = share_ref[pl.ds(k, 1)]
+
+    @pl.when(z > 0)
+    def _():
+        halo_copy(1).wait_recv()
+
+    @pl.when(z < n - 1)
+    def _():
+        halo_copy(0).wait_recv()
+
+    lax.fori_loop(0, 2, at_edge, 0)
+    for load in expert_loads:
+        load.start()
 
     def activate_block(s):
         others = stats.at[pl.ds(0, tp - 1), s]
@@ -647,9 +647,6 @@
         kept[piece, col(c)] = (
             kept[piece, col(c)].astype(jnp.float32) + acc[c, piece]
         ).astype(jnp.bfloat16)
-        pltpu.make_async_copy(
-            kept.at[piece, col(c)], out_hbm.at[piece, col(c)], out_sem.at[0]
-        ).start()
 
     for c in range(PARTS):
         for h in range(SPLIT):
@@ -663,7 +660,6 @@
         return carry
 
     lax.fori_loop(0, n, drain, 0)
-    pltpu.make_async_copy(kept, out_hbm, out_sem.at[0]).wait()
     others = stats.at[pl.ds(0, tp - 1)]
     pltpu.make_async_copy(others, others, stat_send.at[0]).wait()
     for e in range(q_count):
@@ -710,71 +706,70 @@
     spots = max(n + 1, 2 * chans // rows + q_count - 1)
     dma = pltpu.SemaphoreType.DMA
     bf16, f32 = jnp.bfloat16, jnp.float32
-    anywhere = pl.BlockSpec(memory_space=pl.ANY)
+    hbm = pl.BlockSpec(memory_space=pltpu.HBM)
     vmem = pltpu.VMEM
+    scratch = [
+        vmem((block, chans), bf16),
+        vmem((block, chans), bf16),
+        vmem((taps_count, chans), f32),
+        vmem((1, chans), f32),
+        vmem((1, width), f32),
+        vmem((top_count, rows), jnp.int32),
+        vmem((top_count, rows), f32),
+        vmem((block + 2 * edge, chans), bf16),
+        vmem((8, rows // 2 + 2 * edge, chans), f32),
+        vmem((tp, rows, chans), f32),
+        vmem((tp, tp, 8, rows), f32),
+        vmem((q_count, rows, chans), bf16),
+        vmem((q_count, 2, rows, chans), bf16),
+        vmem((q_count - 1, PARTS, rows, cols), bf16),
+        vmem((n, PARTS, rows, cols), bf16),
+        vmem((n, 8, rows), f32),
+        vmem((2, PARTS, slots, cols), bf16),
+        vmem((2, PARTS, slots, cols), bf16),
+        vmem((PAGES, PARTS, slots, cols), bf16),
+        vmem((PAGES, PARTS, slots, cols), bf16),
+        vmem((spots, PARTS, rows, cols), bf16),
+        vmem((PARTS, rows, cols), f32),
+        vmem((width, hidden_width), bf16),
+        vmem((width, hidden_width), bf16),
+        vmem((hidden_width, width), bf16),
+        vmem((slots // groups, hidden_width), f32),
+        vmem((slots // groups, hidden_width), f32),
+        vmem((slots // groups, hidden_width), bf16),
+        dma((8,)),
+        dma((1,)),
+        dma((3,)),
+        dma((2,)),
+        dma((2,)),
+        dma((1,)),
+        dma((tp,)),
+        dma((1,)),
+        dma((1,)),
+        dma((q_count,)),
+        dma((q_count,)),
+        dma((q_count - 1,)),
+        dma((q_count - 1, len(BANDS) - 1)),
+        dma((2, n)),
+        dma((n, len(BANDS) - 1)),
+        dma((2, n)),
+        dma((n,)),
+        dma((2,)),
+        dma((PAGES, groups, PARTS)),
+        dma((2,)),
+        dma((PAGES, groups, PARTS)),
+        dma((n,)),
+        dma((n + 1, PARTS, SPLIT)),
+        pltpu.SemaphoreType.REGULAR,
+    ]
     return pl.pallas_call(
         functools.partial(layer_kernel, n, tp, taps_count, cap),
-        out_shape=jax.ShapeDtypeStruct((rows, width), bf16),
-        in_specs=[anywhere] * 12,
-        out_specs=anywhere,
-        scratch_shapes=[
-            vmem((block, chans), bf16),
-            vmem((block, chans), bf16),
-            vmem((taps_count, chans), f32),
-            vmem((1, chans), f32),
-            vmem((1, width), f32),
-            vmem((top_count, rows), jnp.int32),
-            vmem((top_count, rows), f32),
-            vmem((rows, width), bf16),
-            vmem((block + 2 * edge, chans), bf16),
-            vmem((8, rows // 2 + 2 * edge, chans), f32),
-            vmem((tp, rows, chans), f32),
-            vmem((tp, tp, 8, rows), f32),
-            vmem((q_count, rows, chans), bf16),
-            vmem((q_count, 2, rows, chans), bf16),
-            vmem((q_count - 1, PARTS, rows, cols), bf16),
-            vmem((n, PARTS, rows, cols), bf16),
-            vmem((n, 8, rows), f32),
-            vmem((2, PARTS, slots, cols), bf16),
-            vmem((2, PARTS, slots, cols), bf16),
-            vmem((PAGES, PARTS, slots, cols), bf16),
-            vmem((PAGES, PARTS, slots, cols), bf16),
-            vmem((spots, PARTS, rows, cols), bf16),
-            vmem((PARTS, rows, cols), f32),
-            vmem((width, hidden_width), bf16),
-            vmem((width, hidden_width), bf16),
-            vmem((hidden_width, width), bf16),
-            vmem((slots // groups, hidden_width), f32),
-            vmem((slots // groups, hidden_width), f32),
-            vmem((slots // groups, hidden_width), bf16),
-            dma((8,)),
-            dma((1,)),
-            dma((3,)),
-            dma((1,)),
-            dma((2,)),
-            dma((2,)),
-            dma((1,)),
-            dma((tp,)),
-            dma((1,)),
-            dma((1,)),
-            dma((q_count,)),
-            dma((q_count,)),
-            dma((q_count - 1,)),
-            dma((q_count - 1, len(BANDS) - 1)),
-            dma((2, n)),
-            dma((n, len(BANDS) - 1)),
-            dma((2, n)),
-            dma((n,)),
-            dma((2,)),
-            dma((PAGES, groups, PARTS)),
-            dma((2,)),
-            dma((PAGES, groups, PARTS)),
-            dma((n,)),
-            dma((n + 1, PARTS, SPLIT)),
-            pltpu.SemaphoreType.REGULAR,
-        ],
+        out_shape=vmem((rows, width), bf16),
+        in_specs=[hbm] * 12,
+        out_specs=pl.BlockSpec(memory_space=pltpu.VMEM),
+        scratch_shapes=scratch,
         compiler_params=pltpu.CompilerParams(
-            collective_id=0, has_side_effects=True, vmem_limit_bytes=67043328
+            collective_id=0, has_side_effects=True, vmem_limit_bytes=67043328 - 4 * rows * width
         ),
         name="layer",
     )(

time: 89.2 us -> 87.1 us (0.976)
  local copies, waits for them, and re-layouts: 1.88 us -> 0.8 us
  Pallas kernels: 87.1 us -> 86.2 us
    unnamed x1, local copies, waits for them, and re-layouts: 1.88 us -> 0.8 us
    pallas_call x1, Pallas kernels: 87.1 us -> 86.2 us  [shards(): pl.pallas_call(functools.partial(layer_kernel, n, tp, taps_count, cap), o...]
where the time goes in v4:
time: 87.1 us; the launch traced here: 87 us
  Pallas kernels  86.2 us (99%)
    pallas_call x1, Pallas kernels, shards(): pl.pallas_call(functools.partial(layer_kernel, n, tp, taps_count, cap), o...  86.2 us

profile of v4, /device:TPU:0, one launch (start us, length us, event | category | flops | bytes accessed | tf_op | source)
XLA Modules:
  0.0 87.0 jit_solution(15622302799605217817)
XLA Ops:
  0.0 86.2 %layer.1 = bf16[128,2048]{1,0:T(8,128)(2,1)S(1)} custom-call(bf16[512,256]{1,0:T(8,128)(2,1)} %value_hbm.1, bf16[512,256]{1,0:T(8,128)(2,1)} %gate_hbm.1, f32[31,256]{1,0:T(8,128)} %taps_hbm.1, f32[1,256]{1,0:T(1,128)} %bitcast.5, bf16[256,2048]{1,0:T(8,128)(2,1)} %weight_hbm.1, bf16[128,2048]{1,0:T(8,128)(2,1)} %latent_hbm.1, f32[1,2048]{1,0:T(1,128)} %bitcast.4, ...), custom_call_target="tpu_custom_call" | custom-call | tf_op jit(solution)/shard_map/layer/pallas_call | solution.py:765
  86.2 0.8 copy.14

commit v5 on v4

--- a/solution.py
+++ b/solution.py
@@ -115,42 +115,6 @@
         gate = gate_ref[pl.ds(r, step)].astype(jnp.float32)
         gated[pl.ds(edge + r, step)] = (value * jax.nn.sigmoid(gate)).astype(jnp.bfloat16)
 
-    peers = tp - 1 + (z > 0).astype(jnp.int32) + (z < n - 1).astype(jnp.int32)
-    pl.semaphore_wait(barrier, peers)
-
-    def halo_copy(up):
-        start = block if up else edge
-        place = 0 if up else edge + block
-        return pltpu.make_async_remote_copy(
-            src_ref=gated.at[pl.ds(start, edge)], dst_ref=gated.at[pl.ds(place, edge)],
-            send_sem=halo_send.at[up], recv_sem=halo_recv.at[up],
-            device_id={"sp": z + 1 if up else z - 1}, device_id_type=MESH,
-        )
-
-    @pl.when(z < n - 1)
-    def _():
-        halo_copy(1).start()
-
-    @pl.when(z > 0)
-    def _():
-        halo_copy(0).start()
-
-    own_rows = pl.ds(core * chunks, chunks)
-    pltpu.make_async_copy(inc.at[own_rows], inc.at[own_rows], point_sem.at[0]).wait()
-    mate_copy = pltpu.make_async_remote_copy(
-        src_ref=inc.at[own_rows], dst_ref=inc.at[own_rows],
-        send_sem=mate_send.at[0], recv_sem=mate_recv.at[0],
-        device_id={"tp": mate}, device_id_type=MESH,
-    )
-    mate_copy.start()
-
-    expert_loads = [
-        pltpu.make_async_copy(a, b, w_sem.at[i])
-        for i, (a, b) in enumerate(((wg_hbm.at[0], wg), (wu_hbm.at[0], wu), (wd_hbm.at[0], wd)))
-    ]
-    for load in loads[2:]:
-        load.wait()
-
     tile = rows // 2
 
     def convolve(s, r):
@@ -163,6 +127,47 @@
             a, b = divmod(edge - half + i, 8)
             value = value + taps_ref[pl.ds(i, 1)] * wide[b, pl.ds(8 * a, tile)]
         mixed[s, pl.ds(pl.multiple_of(r, 16), tile)] = value
+
+    opening = jnp.where(quad == 0, 2, 1)
+    loads[2].wait()
+    convolve(opening, 0)
+    convolve(opening, tile)
+
+    peers = tp - 1 + (z > 0).astype(jnp.int32) + (z < n - 1).astype(jnp.int32)
+    pl.semaphore_wait(barrier, peers)
+
+    def halo_copy(up):
+        start = block if up else edge
+        place = 0 if up else edge + block
+        return pltpu.make_async_remote_copy(
+            src_ref=gated.at[pl.ds(start, edge)], dst_ref=gated.at[pl.ds(place, edge)],
+            send_sem=halo_send.at[up], recv_sem=halo_recv.at[up],
+            device_id={"sp": z + 1 if up else z - 1}, device_id_type=MESH,
+        )
+
+    @pl.when(z < n - 1)
+    def _():
+        halo_copy(1).start()
+
+    @pl.when(z > 0)
+    def _():
+        halo_copy(0).start()
+
+    own_rows = pl.ds(core * chunks, chunks)
+    pltpu.make_async_copy(inc.at[own_rows], inc.at[own_rows], point_sem.at[0]).wait()
+    mate_copy = pltpu.make_async_remote_copy(
+        src_ref=inc.at[own_rows], dst_ref=inc.at[own_rows],
+        send_sem=mate_send.at[0], recv_sem=mate_recv.at[0],
+        device_id={"tp": mate}, device_id_type=MESH,
+    )
+    mate_copy.start()
+
+    expert_loads = [
+        pltpu.make_async_copy(a, b, w_sem.at[i])
+        for i, (a, b) in enumerate(((wg_hbm.at[0], wg), (wu_hbm.at[0], wu), (wd_hbm.at[0], wd)))
+    ]
+    for load in loads[3:]:
+        load.wait()
 
     def measure(s):
         value = mixed[s]
@@ -177,7 +182,7 @@
             ).start()
 
     def inner(i, carry):
-        s = jnp.where(quad == 0, tp - 2 - i, i + 1)
+        s = jnp.where(i == 1, 3 - opening, i + 1)
         convolve(s, 0)
         convolve(s, tile)
         measure(s)
@@ -193,7 +198,8 @@
         measure(side * (tp - 1))
         return carry
 
-    lax.fori_loop(0, tp - 2, inner, 0)
+    measure(opening)
+    lax.fori_loop(1, tp - 2, inner, 0)
     lax.fori_loop(0, 2, near_edge, 0)
 
     ids = ids_ref[...].astype(jnp.float32)
@@ -212,18 +218,6 @@
         tabs[z, pl.ds(k, 1)] = ids[k : k + 1] * cap + count
         tabs[z, pl.ds(top_count + k, 1)] = share_ref[pl.ds(k, 1)]
 
-    @pl.when(z > 0)
-    def _():
-        halo_copy(1).wait_recv()
-
-    @pl.when(z < n - 1)
-    def _():
-        halo_copy(0).wait_recv()
-
-    lax.fori_loop(0, 2, at_edge, 0)
-    for load in expert_loads:
-        load.start()
-
     def activate_block(s):
         others = stats.at[pl.ds(0, tp - 1), s]
         pltpu.make_async_copy(others, others, stat_recv.at[s]).wait()
@@ -248,6 +242,30 @@
             device_id={"tp": mate}, device_id_type=MESH,
         )
 
+    def share_block(s):
+        @pl.when(lax.rem(s, 2) == core)
+        def _():
+            act_in[s // 2, core] = activate_block(s)
+
+        @pl.when(lax.rem(s, 2) != core)
+        def _():
+            act_out[s // 2] = activate_block(s)
+            act_copy(s // 2).start()
+
+    share_block(opening)
+
+    @pl.when(z > 0)
+    def _():
+        halo_copy(1).wait_recv()
+
+    @pl.when(z < n - 1)
+    def _():
+        halo_copy(0).wait_recv()
+
+    lax.fori_loop(0, 2, at_edge, 0)
+    for load in expert_loads:
+        load.start()
+
     def product(spot, c):
         left = jnp.concatenate([act_in[spot, 0], act_in[spot, 1]], axis=1)
         right = inc[pl.ds(0, base), c].reshape(base * rows, cols)
@@ -262,33 +280,11 @@
             device_id={"tp": 2 * spot + core}, device_id_type=MESH,
         )
 
-    for e in range(q_count):
-        theirs, ours = spot_of(e, 1 - core), spot_of(e, core)
-        act_out[theirs] = activate_block(2 * theirs + 1 - core)
-        act_copy(theirs).start()
-        act_in[ours, core] = activate_block(2 * ours + core)
-        if e == 0:
-            mate_copy.wait()
-        pltpu.make_async_copy(act_out.at[ours], act_out.at[ours], act_recv.at[ours]).wait()
-
-        @pl.when(ours != quad)
-        def _():
-            i = lax.rem(ours - quad + q_count, q_count) - 1
-            for c in range(PARTS):
-                psend[i, c] = product(ours, c).astype(jnp.bfloat16)
-            for k in range(len(BANDS) - 1):
-                part_copy(ours, k).start()
-
-        @pl.when(ours == quad)
-        def _():
-            for c in range(PARTS):
-                acc[c] = product(ours, c)
-
     def token_copy(zs, k, side):
         piece = band(k)
         return pltpu.make_async_remote_copy(
             src_ref=toks.at[zs, :, piece], dst_ref=toks.at[zs, :, piece],
-            send_sem=tok_send.at[side, zs], recv_sem=tok_recv.at[zs, k],
+            send_sem=tok_send.at[side, zs], recv_sem=tok_recv.at[zs, k // 2],
             device_id={"sp": z + 1 if side else z - 1}, device_id_type=MESH,
         )
 
@@ -308,9 +304,7 @@
         def _():
             act(0)
 
-    each_side(z, lambda side: table_copy(z, side).start())
-
-    for k in range(len(BANDS) - 1):
+    def send_band(k):
         piece = band(k)
         for i in range(1, q_count):
             spot = inc.at[base + i - 1, :, piece]
@@ -330,6 +324,34 @@
             toks[z, c, piece] = (after * norm * gain_ref[:, col(c)]).astype(jnp.bfloat16)
         each_side(z, lambda side: token_copy(z, k, side).start())
 
+    for e in range(q_count):
+        theirs, ours = spot_of(e, 1 - core), spot_of(e, core)
+        if e == 0:
+            share_block(3 - opening)
+            mate_copy.wait()
+        else:
+            act_out[theirs] = activate_block(2 * theirs + 1 - core)
+            act_copy(theirs).start()
+            act_in[ours, core] = activate_block(2 * ours + core)
+        pltpu.make_async_copy(act_out.at[ours], act_out.at[ours], act_recv.at[ours]).wait()
+
+        @pl.when(ours != quad)
+        def _():
+            i = lax.rem(ours - quad + q_count, q_count) - 1
+            for c in range(PARTS):
+                psend[i, c] = product(ours, c).astype(jnp.bfloat16)
+            for k in range(len(BANDS) - 1):
+                part_copy(ours, k).start()
+
+        @pl.when(ours == quad)
+        def _():
+            for c in range(PARTS):
+                acc[c] = product(ours, c)
+
+    each_side(z, lambda side: table_copy(z, side).start())
+    for k in range(len(BANDS) - 1):
+        send_band(k)
+
 
     upper = z > n - 1 - z
     middle = (z > 0) & (z < n - 1)
@@ -359,7 +381,7 @@
                 src_ref=from_ref.at[side, c, span(g, other)],
                 dst_ref=to_ref.at[page, c, span(g, t)],
                 send_sem=ss.at[side],
-                recv_sem=rs.at[page, g, c],
+                recv_sem=rs.at[page, g, c] if to_ref is arr else rs.at[page, c],
                 device_id={"tp": other},
                 device_id_type=MESH,
             ).start()
@@ -402,8 +424,8 @@
         return ((zs < z) & (z < n - 1)) | ((zs > z) & (z > 0))
 
     def arrive(zs, k):
-        spot = toks.at[zs, :, band(k)]
-        pltpu.make_async_copy(spot, spot, tok_recv.at[zs, k]).wait()
+        spot = toks.at[zs, :, pl.ds(band(k).start, band(k).size + band(k + 1).size)]
+        pltpu.make_async_copy(spot, spot, tok_recv.at[zs, k // 2]).wait()
 
     def wait_passed(zs, side):
         table_copy(zs, side).wait_send()
@@ -423,7 +445,8 @@
             pltpu.make_async_copy(tabs.at[zs], tabs.at[zs], tab_recv.at[zs]).wait()
             each_side(zs, lambda side: table_copy(zs, side).start())
             for k in range(len(BANDS) - 1):
-                arrive(zs, k)
+                if k % 2 == 0:
+                    arrive(zs, k)
                 each_side(zs, lambda side: token_copy(zs, k, side).start())
 
     def take(j):
@@ -432,7 +455,7 @@
         @pl.when((zs != z) & jnp.logical_not(passes_on(zs)))
         def _():
             pltpu.make_async_copy(tabs.at[zs], tabs.at[zs], tab_recv.at[zs]).wait()
-            for k in range(len(BANDS) - 1):
+            for k in range(0, len(BANDS) - 1, 2):
                 arrive(zs, k)
 
         first, second, _ = names(zs)
@@ -497,8 +520,8 @@
 
         each_side(zs, sent)
         for c in range(PARTS):
-            for g in range(groups):
-                wait_pieces(back, page, g, c, back_recv)
+            part = back.at[page, c, pl.ds(0, (tp - 1) * cap)]
+            pltpu.make_async_copy(part, part, back_recv.at[page, c]).wait()
             value = jnp.dot(high, back[page, c], preferred_element_type=jnp.float32) + jnp.dot(
                 rest, back[page, c], preferred_element_type=jnp.float32
             )
@@ -751,13 +774,13 @@
         dma((q_count - 1,)),
         dma((q_count - 1, len(BANDS) - 1)),
         dma((2, n)),
-        dma((n, len(BANDS) - 1)),
+        dma((n, (len(BANDS) - 1) // 2)),
         dma((2, n)),
         dma((n,)),
         dma((2,)),
         dma((PAGES, groups, PARTS)),
         dma((2,)),
-        dma((PAGES, groups, PARTS)),
+        dma((PAGES, PARTS)),
         dma((n,)),
         dma((n + 1, PARTS, SPLIT)),
         pltpu.SemaphoreType.REGULAR,

time: 87.1 us -> 86 us (0.987)
  Pallas kernels: 86.2 us -> 85.1 us
    pallas_call x1, Pallas kernels: 86.2 us -> 85.1 us  [shards(): pl.pallas_call(functools.partial(layer_kernel, n, tp, taps_count, cap), o...]
where the time goes in v5:
time: 86 us; the launch traced here: 85.9 us
  Pallas kernels  85.1 us (99%)
    pallas_call x1, Pallas kernels, shards(): pl.pallas_call(functools.partial(layer_kernel, n, tp, taps_count, cap), o...  85.1 us

profile of v5, /device:TPU:0, one launch (start us, length us, event | category | flops | bytes accessed | tf_op | source)
XLA Modules:
  0.0 85.9 jit_solution(6851940970286991557)
XLA Ops:
  0.0 85.1 %layer.1 = bf16[128,2048]{1,0:T(8,128)(2,1)S(1)} custom-call(bf16[512,256]{1,0:T(8,128)(2,1)} %value_hbm.1, bf16[512,256]{1,0:T(8,128)(2,1)} %gate_hbm.1, f32[31,256]{1,0:T(8,128)} %taps_hbm.1, f32[1,256]{1,0:T(1,128)} %bitcast.5, bf16[256,2048]{1,0:T(8,128)(2,1)} %weight_hbm.1, bf16[128,2048]{1,0:T(8,128)(2,1)} %latent_hbm.1, f32[1,2048]{1,0:T(1,128)} %bitcast.4, ...), custom_call_target="tpu_custom_call" | custom-call | tf_op jit(solution)/shard_map/layer/pallas_call | solution.py:788
  85.1 0.8 copy.14

commit v6 on v5

--- a/solution.py
+++ b/solution.py
@@ -586,7 +586,7 @@
         return middle & (turn > 0) & up & down
 
     pieces = PARTS * SPLIT
-    early_stops = (pieces // 4, pieces // 2 + 1, pieces + LAG)
+    early_stops = (pieces // 8, pieces // 2, pieces + LAG)
 
     def early_relays(turn, stop):
         start = (0,) + early_stops

time: 86 us -> 86 us (level)
  no operation moved by 1% of the time
where the time goes in v6:
time: 86 us; the launch traced here: 85.9 us
  Pallas kernels  85.1 us (99%)
    pallas_call x1, Pallas kernels, shards(): pl.pallas_call(functools.partial(layer_kernel, n, tp, taps_count, cap), o...  85.1 us

profile of v6, /device:TPU:0, one launch (start us, length us, event | category | flops | bytes accessed | tf_op | source)
XLA Modules:
  0.0 85.9 jit_solution(13313335751079233517)
XLA Ops:
  0.0 85.1 %layer.1 = bf16[128,2048]{1,0:T(8,128)(2,1)S(1)} custom-call(bf16[512,256]{1,0:T(8,128)(2,1)} %value_hbm.1, bf16[512,256]{1,0:T(8,128)(2,1)} %gate_hbm.1, f32[31,256]{1,0:T(8,128)} %taps_hbm.1, f32[1,256]{1,0:T(1,128)} %bitcast.5, bf16[256,2048]{1,0:T(8,128)(2,1)} %weight_hbm.1, bf16[128,2048]{1,0:T(8,128)(2,1)} %latent_hbm.1, f32[1,2048]{1,0:T(1,128)} %bitcast.4, ...), custom_call_target="tpu_custom_call" | custom-call | tf_op jit(solution)/shard_map/layer/pallas_call | solution.py:788
  85.1 0.8 copy.14
